TPU v7x, 128 devices: a whole 4x4x4 slice. The times are simulated.
128 devices in a mesh: sp: 16 (over z, x), tp: 8 (over y, core).
Axes of the slice: x: 4, y: 4, z: 4, core: 2. Of those that a mesh axis runs over, the one named last changes fastest.
Arguments:
- latent: bfloat16 [8192, 4096], P('sp'), may hold values from -64 to 64
- context: bfloat16 [1024, 4096], P('sp'), may hold values from -6 to 6
- condition: bfloat16 [4096], P('sp'), may hold values from -6 to 6
- context_condition: bfloat16 [4096], P('sp'), may hold values from -6 to 6
- shift_weight: bfloat16 [4096, 4096], P('sp', 'tp'), may hold values from -0.125 to 0.125
- scale_weight: bfloat16 [4096, 4096], P('sp', 'tp'), may hold values from -0.125 to 0.125
- gate_weight: bfloat16 [4096, 4096], P('sp', 'tp'), may hold values from -0.25 to 0.25
- norm_gain: float32 [4096], replicated, may hold values from 0.1 to 1.9
- query_weight: bfloat16 [4096, 2048], P(None, 'tp'), may hold values from -0.09375 to 0.09375
- key_weight: bfloat16 [4096, 2048], P(None, 'tp'), may hold values from -0.09375 to 0.09375
- value_weight: bfloat16 [4096, 2048], P(None, 'tp'), may hold values from -0.09375 to 0.09375
- write_weight: bfloat16 [4096, 2, 16], replicated, may hold values from -0.09375 to 0.09375
- decay_weight: bfloat16 [4096, 2, 16], replicated, may hold values from -0.09375 to 0.09375
- write_bias: float32 [2, 16], replicated, may hold values from -12 to 1
- decay_bias: float32 [2, 16], replicated, may hold values from -16 to -4
- log_rate: float32 [2, 16], replicated, may hold values from 0 to 1.4
- head_gain: float32 [128], replicated, may hold values from 0.1 to 1.9
- out_weight: bfloat16 [2048, 4096], P(None, 'tp'), may hold values from -0.125 to 0.125
Outputs:
- updated: bfloat16 [8192, 4096], P('sp', 'tp')
All inputs are finite; a program needn't handle non-finite values.
Results may differ from a plain program's by a relative error of at most 0.013.
Values may be sent and summed in bfloat16 or wider, within the bound.
A program may use at most 128 MiB of HBM per device.

v0:
```python
import functools

import jax
import jax.numpy as jnp
from jax import lax
from jax.experimental import pallas as pl
from jax.experimental.pallas import tpu as pltpu
from jax.sharding import PartitionSpec as P

HEAD_DIM = 128
CHUNK = 128
epsilon = 0.0001
bf16 = jnp.bfloat16
f32 = jnp.float32


def mm(a, b):
    return jnp.dot(a.astype(bf16), b.astype(bf16), preferred_element_type=f32)


def spans(tokens, ctx_tokens):
    size = min(CHUNK, tokens)
    lat = [(at, size) for at in range(0, tokens, size)]
    ctx_size = min(CHUNK, ctx_tokens)
    ctx = [(tokens + at, ctx_size) for at in range(0, ctx_tokens, ctx_size)]
    return lat, ctx


def prep_kernel(tokens, ctx_tokens, q_ref, k_ref, v_ref, col_ref, row_ref, o_ref, e_ref, map_ref):
    lat, ctx = spans(tokens, ctx_tokens)
    items = []
    shared = {}
    for at, size in lat + ctx:
        keys = k_ref[at : at + size, :]
        keys_t = keys.astype(f32).T
        gram = jnp.dot(keys, keys_t.astype(bf16), preferred_element_type=f32)
        rows = lax.broadcasted_iota(jnp.int32, (size, size), 0)
        cols = lax.broadcasted_iota(jnp.int32, (size, size), 1)
        diag = jnp.where(rows == cols, gram, 0.0)
        s_col = lax.rsqrt(jnp.sum(diag, axis=1, keepdims=True) + epsilon)
        s_row = lax.rsqrt(jnp.sum(diag, axis=0, keepdims=True) + epsilon)
        gram = gram * s_col * s_row
        entry = dict(keys=keys.astype(f32) * s_col, keys_t=keys_t * s_row, values=v_ref[at : at + size, :].astype(f32))
        if at < tokens:
            queries = q_ref[at : at + size, :].astype(f32)
            q_scale = lax.rsqrt(jnp.sum(queries * queries, axis=1, keepdims=True) + epsilon) * HEAD_DIM**-0.5
            entry["queries"] = queries * q_scale
            entry["score"] = (
                jnp.dot(q_ref[at : at + size, :], keys_t.astype(bf16), preferred_element_type=f32) * q_scale * s_row
            )
        shared[at] = entry
        for d in range(2):
            rate_col = col_ref[0, at : at + size, 2 * d : 2 * d + 1]
            run_col = col_ref[0, at : at + size, 2 * d + 1 : 2 * d + 2]
            run_row = row_ref[0, 2 * d + 1 : 2 * d + 2, at : at + size]
            inside = rows >= cols if d == 0 else rows <= cols
            strict = rows > cols if d == 0 else rows < cols
            decay = jnp.where(inside, jnp.exp(jnp.minimum(run_col - run_row, 0.0)), 0.0)
            system = jnp.where(strict, gram * decay * rate_col, 0.0)
            item = dict(at=at, size=size, d=d, rate_col=rate_col, run_col=run_col, run_row=run_row)
            item["system"] = system
            if at < tokens:
                item["score"] = entry["score"] * decay
            near = (rows // 2) == (cols // 2)
            item["inv"] = jnp.where(rows == cols, 1.0, jnp.where(near, -system, 0.0))
            items.append(item)
    span = 2
    while span < max(item["size"] for item in items):
        firsts = []
        for item in items:
            if span >= item["size"]:
                firsts.append(None)
                continue
            size = item["size"]
            rows = lax.broadcasted_iota(jnp.int32, (size, size), 0) // span
            cols = lax.broadcasted_iota(jnp.int32, (size, size), 1) // span
            if item["d"] == 0:
                mask = ((rows % 2) == 1) & (cols == rows - 1)
            else:
                mask = ((cols % 2) == 1) & (rows == cols - 1)
            firsts.append(mm(jnp.where(mask, item["system"], 0.0), item["inv"]))
        for item, first in zip(items, firsts):
            if first is not None:
                item["inv"] = item["inv"] - mm(item["inv"], first)
        span *= 2
    for item in items:
        entry = shared[item["at"]]
        growth = jnp.exp(item["run_col"])
        both = jnp.concatenate(
            [entry["values"] * item["rate_col"], entry["keys"] * (item["rate_col"] * growth)], axis=1
        )
        item["solved"] = mm(item["inv"], both)
        last = item["run_row"][:, item["size"] - 1 :] if item["d"] == 0 else item["run_row"][:, :1]
        item["gate"] = jnp.exp(last)
        late_t = entry["keys_t"] * jnp.exp(last - item["run_row"])
        item["late"] = mm(late_t, item["solved"])
        if item["at"] < tokens:
            weighed = mm(item["score"], item["solved"])
            item["local"] = weighed[:, :HEAD_DIM]
            item["early"] = entry["queries"] * growth - weighed[:, HEAD_DIM:]
    eye_r = lax.broadcasted_iota(jnp.int32, (HEAD_DIM, HEAD_DIM), 0)
    eye_c = lax.broadcasted_iota(jnp.int32, (HEAD_DIM, HEAD_DIM), 1)
    eye = (eye_r == eye_c).astype(f32)

    def chain(chunks, d, emit):
        carry = None
        for item in chunks if d == 0 else chunks[::-1]:
            if emit:
                if carry is None:
                    out, early = item["local"], item["early"]
                else:
                    moved = mm(item["early"], carry)
                    out = item["local"] + moved[:, :HEAD_DIM]
                    early = item["early"] + moved[:, HEAD_DIM:]
                e_ref[0, item["at"] : item["at"] + item["size"], d * HEAD_DIM : (d + 1) * HEAD_DIM] = early.astype(
                    bf16
                )
                item["out"] = out
            late, gate = item["late"], item["gate"]
            fresh = jnp.concatenate([late[:, :HEAD_DIM], (gate - 1.0) * eye - late[:, HEAD_DIM:]], axis=1)
            if carry is None:
                carry = fresh
            else:
                carry = gate * carry + fresh - mm(late[:, HEAD_DIM:], carry)
        return carry

    for d in range(2):
        latents = [i for i in items if i["d"] == d and i["at"] < tokens]
        contexts = [i for i in items if i["d"] == d and i["at"] >= tokens]
        map_ref[0, d] = chain(contexts, d, False).astype(bf16)
        map_ref[1, d] = chain(latents, d, True).astype(bf16)
    for at, size in lat:
        pair = [i for i in items if i["at"] == at]
        o_ref[0, at : at + size, :] = pair[0]["out"] + pair[1]["out"]


def apply_maps(maps, state):
    high = state.astype(bf16)
    low = (state - high.astype(f32)).astype(bf16)
    move = maps[:, HEAD_DIM:]
    return (
        state
        + maps[:, :HEAD_DIM].astype(f32)
        + jnp.dot(move, high, preferred_element_type=f32)
        + jnp.dot(move, low, preferred_element_type=f32)
    )


def on_mesh(sp=None, tp=None):
    return (lax.axis_index("sp") if sp is None else sp, lax.axis_index("tp") if tp is None else tp)


def send(src, dst, send_sem, recv_sem, device):
    return pltpu.make_async_remote_copy(
        src_ref=src,
        dst_ref=dst,
        send_sem=send_sem,
        recv_sem=recv_sem,
        device_id=device,
        device_id_type=pl.DeviceIdType.MESH,
    )


def greet(devices):
    barrier = pltpu.get_barrier_semaphore()
    for device in devices:
        pl.semaphore_signal(barrier, inc=1, device_id=device, device_id_type=pl.DeviceIdType.MESH)


def modulation_kernel(
    sp, tp, silu_ref, shift_ref, scale_ref, gate_ref, rows_ref, gate_out, got, blocks, sent_a, recv_a, sent_b, recv_b
):
    me, col = lax.axis_index("sp"), lax.axis_index("tp")
    width = shift_ref.shape[1]
    rings = [on_mesh(sp=lax.rem(me + r, sp)) for r in range(1, sp)]
    cross = [on_mesh(tp=lax.rem(col + r, tp)) for r in range(1, tp)]
    greet(rings + cross)
    silu = silu_ref[...]
    shift = jnp.dot(silu, shift_ref[...], preferred_element_type=f32)
    scale = jnp.dot(silu, scale_ref[...], preferred_element_type=f32)
    gate = jnp.dot(silu, gate_ref[...], preferred_element_type=f32)
    got[me] = jnp.concatenate([shift[0:2], scale[0:2], gate[0:1], jnp.zeros((3, width), f32)], axis=0)
    pl.semaphore_wait(pltpu.get_barrier_semaphore(), len(rings) + len(cross))
    out = []
    for r, device in enumerate(rings):
        out.append(send(got.at[me], got.at[me], sent_a.at[r], recv_a.at[me], device))
        out[-1].start()
    for r in range(1, sp):
        src = lax.rem(me + r, sp)
        send(got.at[src], got.at[src], sent_a.at[0], recv_a.at[src], on_mesh(sp=src)).wait_recv()
    total = got[0]
    for place in range(1, sp):
        total = total + got[place]
    blocks[col] = total
    gate_out[...] = total[4:5]
    for r, device in enumerate(cross):
        out.append(send(blocks.at[col], blocks.at[col], sent_b.at[r], recv_b.at[col], device))
        out[-1].start()
    for r in range(1, tp):
        src = lax.rem(col + r, tp)
        send(blocks.at[src], blocks.at[src], sent_b.at[0], recv_b.at[src], on_mesh(tp=src)).wait_recv()
    for place in range(tp):
        rows_ref[:, place * width : (place + 1) * width] = blocks[place][0:4]
    for copy in out:
        copy.wait_send()


def modulation(silu_rows, shift_weight, scale_weight, gate_weight):
    sp, tp = lax.axis_size("sp"), lax.axis_size("tp")
    width = shift_weight.shape[1]
    vmem = pl.BlockSpec(memory_space=pltpu.VMEM)
    return pl.pallas_call(
        functools.partial(modulation_kernel, sp, tp),
        in_specs=[vmem] * 4,
        out_specs=[vmem] * 2,
        out_shape=[jax.ShapeDtypeStruct((4, tp * width), f32), jax.ShapeDtypeStruct((1, width), f32)],
        scratch_shapes=[
            pltpu.VMEM((sp, 8, width), f32),
            pltpu.VMEM((tp, 8, width), f32),
            pltpu.SemaphoreType.DMA((sp,)),
            pltpu.SemaphoreType.DMA((sp,)),
            pltpu.SemaphoreType.DMA((tp,)),
            pltpu.SemaphoreType.DMA((tp,)),
        ],
        compiler_params=pltpu.CompilerParams(collective_id=0, has_side_effects=True),
        name="modulation",
    )(jnp.pad(silu_rows, ((0, 6), (0, 0))), shift_weight, scale_weight, gate_weight)


def exchange_kernel(
    sp, per, tokens, ctx_tokens, q_ref, k_ref, v_ref, col_ref, row_ref, gain_ref, out_ref,
    o_ref, e_ref, maps_ref, got, starts, back, sent_a, recv_a, sent_b, recv_b,
):
    me = lax.axis_index("sp")
    heads = col_ref.shape[0]
    items = 2 * heads
    peers = [lax.rem(me + r, sp) for r in range(1, sp)]
    greet([on_mesh(sp=peer) for peer in peers])
    pl.semaphore_wait(pltpu.get_barrier_semaphore(), sp - 1)

    def ship(part, item):
        owner, slot = item // per, lax.rem(item, per)
        return owner, send(
            maps_ref.at[part, item],
            got.at[part, me, slot],
            sent_a.at[part, item],
            recv_a.at[part, me, slot],
            on_mesh(sp=owner),
        )

    def one_head(k, unused):
        head = lax.rem(me * per // 2 + heads // 2 + k + (heads - heads // 2 + 1), heads)
        lanes = pl.ds(pl.multiple_of(head * HEAD_DIM, HEAD_DIM), HEAD_DIM)
        prep_kernel(
            tokens,
            ctx_tokens,
            q_ref.at[:, lanes],
            k_ref.at[:, lanes],
            v_ref.at[:, lanes],
            col_ref.at[pl.ds(head, 1)],
            row_ref.at[pl.ds(head, 1)],
            o_ref.at[pl.ds(head, 1)],
            e_ref.at[pl.ds(head, 1)],
            maps_ref.at[:, pl.ds(2 * head, 2)],
        )
        for d in range(2):
            for part in range(2):
                owner, copy = ship(part, 2 * head + d)

                @pl.when(owner != me)
                def _():
                    copy.start()

                @pl.when(owner == me)
                def _():
                    got[part, me, lax.rem(2 * head + d, per)] = maps_ref[part, 2 * head + d]

        return unused

    lax.fori_loop(0, heads, one_head, 0)

    def arrive(part, slot):
        for peer in peers:
            spot = got.at[part, peer, slot]
            send(spot, spot, sent_a.at[part, 0], recv_a.at[part, peer, slot], on_mesh(sp=peer)).wait_recv()

    def give_back(place, slot):
        return send(
            starts.at[place, slot],
            back.at[me, slot],
            sent_b.at[place, slot],
            recv_b.at[me, slot],
            on_mesh(sp=place),
        )

    for slot in range(per):

        @pl.when(me * per + slot < items)
        def _():
            reverse = lax.rem(me * per + slot, 2)
            arrive(0, slot)
            state = jnp.zeros((HEAD_DIM, HEAD_DIM), f32)
            for step in range(sp):
                state = apply_maps(got[0, step + reverse * (sp - 1 - 2 * step), slot], state)
            arrive(1, slot)
            for step in range(sp):
                place = step + reverse * (sp - 1 - 2 * step)
                starts[place, slot] = state.astype(bf16)

                @pl.when(place != me)
                def _():
                    give_back(place, slot).start()

                @pl.when(place == me)
                def _():
                    back[me, slot] = starts[me, slot]

                if step < sp - 1:
                    state = apply_maps(got[1, place, slot], state)

    for item in range(items):
        owner, slot = item // per, item % per

        @pl.when(owner != me)
        def _():
            spot = back.at[owner, slot]
            send(spot, spot, sent_b.at[owner, slot], recv_b.at[owner, slot], on_mesh(sp=owner)).wait_recv()

    for head in range(heads):
        pair = [back[item // per, item % per] for item in (2 * head, 2 * head + 1)]
        combined = o_ref[head] + jnp.dot(
            e_ref[head], jnp.concatenate(pair, axis=0), preferred_element_type=f32
        )
        scale = lax.rsqrt(jnp.mean(combined * combined, axis=1, keepdims=True) + epsilon)
        out_ref[:, head * HEAD_DIM : (head + 1) * HEAD_DIM] = (combined * scale * gain_ref[...]).astype(bf16)
    for item in range(items):
        for part in range(2):
            owner, copy = ship(part, item)

            @pl.when(owner != me)
            def _():
                copy.wait_send()

    for slot in range(per):

        @pl.when(me * per + slot < items)
        def _():
            for peer in peers:
                give_back(peer, slot).wait_send()


def exchange(queries, keys, values, col, row, gain, tokens, ctx_tokens):
    heads = col.shape[0]
    items = 2 * heads
    sp = lax.axis_size("sp")
    per = -(-items // sp)
    vmem = pl.BlockSpec(memory_space=pltpu.VMEM)
    dma = pltpu.SemaphoreType.DMA
    return pl.pallas_call(
        functools.partial(exchange_kernel, sp, per, tokens, ctx_tokens),
        in_specs=[vmem] * 6,
        out_specs=vmem,
        out_shape=jax.ShapeDtypeStruct((tokens, heads * HEAD_DIM), bf16),
        scratch_shapes=[
            pltpu.VMEM((heads, tokens, HEAD_DIM), f32),
            pltpu.VMEM((heads, tokens, 2 * HEAD_DIM), bf16),
            pltpu.VMEM((2, items, HEAD_DIM, 2 * HEAD_DIM), bf16),
            pltpu.VMEM((2, sp, per, HEAD_DIM, 2 * HEAD_DIM), bf16),
            pltpu.VMEM((sp, per, HEAD_DIM, HEAD_DIM), bf16),
            pltpu.VMEM((sp, per, HEAD_DIM, HEAD_DIM), bf16),
            dma((2, items)),
            dma((2, sp, per)),
            dma((sp, per)),
            dma((sp, per)),
        ],
        compiler_params=pltpu.CompilerParams(
            collective_id=1, has_side_effects=True, vmem_limit_bytes=48 * 1024 * 1024
        ),
        name="exchange",
    )(queries, keys, values, col, row, gain)


def output_kernel(
    tp, pieces, head_ref, gate_ref, latent_ref, weight_ref, out_ref,
    got, weight, residual, acc, local_sems, sent_y, recv_y, sent_c, recv_c, sent_r, recv_r,
):
    me, col = lax.axis_index("sp"), lax.axis_index("tp")
    core = lax.rem(col, 2)
    partner = col + 1 - 2 * core
    chips = tp // 2
    far = [lax.rem(col + 2 * r, tp) for r in range(1, chips)]
    far_partner = [place + 1 - 2 * core for place in far]
    tokens, depth = head_ref.shape
    width = out_ref.shape[1]
    rows = tokens // pieces
    load = pltpu.make_async_copy(weight_ref, weight, local_sems.at[0])
    load.start()
    take = pltpu.make_async_copy(
        latent_ref.at[:, pl.ds(pl.multiple_of(col * width, width), width)], residual, local_sems.at[1]
    )
    take.start()
    greet([on_mesh(tp=place) for place in [partner] + far])
    pl.semaphore_wait(pltpu.get_barrier_semaphore(), chips)
    out = []

    def piece(ref, p):
        return ref.at[pl.ds(p * rows, rows)]

    for p in range(pieces):
        for r, place in enumerate(far):
            out.append(
                send(piece(head_ref, p), piece(got.at[col], p), sent_y.at[r, p], recv_y.at[col, p], on_mesh(tp=place))
            )
            out[-1].start()
    for p in range(pieces):
        out.append(
            send(piece(head_ref, p), piece(got.at[col], p), sent_c.at[p], recv_c.at[p], on_mesh(tp=partner))
        )
        out[-1].start()
    load.wait()

    def weights(src):
        return weight[pl.ds(pl.multiple_of(src * depth, depth), depth), :]

    def add(p, block, src, first=False):
        part = jnp.dot(block, weights(src), preferred_element_type=f32)
        at = pl.ds(p * rows, rows)
        acc[at, :] = part if first else acc[at, :] + part

    for p in range(pieces):
        add(p, head_ref[pl.ds(p * rows, rows), :], col, True)
    for p in range(pieces):
        spot = piece(got.at[partner], p)
        send(spot, spot, sent_c.at[p], recv_c.at[p], on_mesh(tp=partner)).wait_recv()
        add(p, spot[...], partner)
    take.wait()
    for p in range(pieces):
        for r, src in enumerate(far):
            spot = piece(got.at[src], p)
            send(spot, spot, sent_y.at[r, p], recv_y.at[src, p], on_mesh(tp=src)).wait_recv()
            out.append(send(spot, spot, sent_r.at[r, p], recv_r.at[src, p], on_mesh(tp=partner)))
            out[-1].start()
            add(p, spot[...], src)
        for r, src in enumerate(far_partner):
            spot = piece(got.at[src], p)
            send(spot, spot, sent_r.at[r, p], recv_r.at[src, p], on_mesh(tp=partner)).wait_recv()
            add(p, spot[...], src)
        at = pl.ds(p * rows, rows)
        out_ref[at, :] = (residual[at, :].astype(f32) + gate_ref[...] * acc[at, :]).astype(bf16)
    for copy in out:
        copy.wait_send()


def output(head_out, gate_row, latent, out_weight):
    tp = lax.axis_size("tp")
    tokens, depth = head_out.shape
    width = out_weight.shape[1]
    pieces = 4
    vmem = pl.BlockSpec(memory_space=pltpu.VMEM)
    anywhere = pl.BlockSpec(memory_space=pl.ANY)
    dma = pltpu.SemaphoreType.DMA
    return pl.pallas_call(
        functools.partial(output_kernel, tp, pieces),
        in_specs=[vmem, vmem, anywhere, anywhere],
        out_specs=vmem,
        out_shape=jax.ShapeDtypeStruct((tokens, width), bf16),
        scratch_shapes=[
            pltpu.VMEM((tp, tokens, depth), bf16),
            pltpu.VMEM(out_weight.shape, bf16),
            pltpu.VMEM((tokens, width), bf16),
            pltpu.VMEM((tokens, width), f32),
            dma((2,)),
            dma((tp, pieces)),
            dma((tp, pieces)),
            dma((pieces,)),
            dma((pieces,)),
            dma((tp, pieces)),
            dma((tp, pieces)),
        ],
        compiler_params=pltpu.CompilerParams(
            collective_id=2, has_side_effects=True, vmem_limit_bytes=63 * 1024 * 1024
        ),
        name="output",
    )(head_out, gate_row, latent, out_weight)


def rms_rows(row_data, row_gain):
    values = row_data.astype(f32)
    scaled = values * lax.rsqrt(jnp.mean(values * values, axis=-1, keepdims=True) + epsilon)
    return scaled * row_gain


def project(matrix, weight):
    return jnp.dot(matrix, weight, preferred_element_type=f32).astype(bf16)


def running_sums(log_decay, size):
    parts = log_decay.reshape((-1, size) + log_decay.shape[1:])
    lower = jnp.tril(jnp.ones((size, size), f32))
    ahead = jnp.einsum("ij,njh->nih", lower, parts[:, :, 0], precision=lax.Precision.HIGHEST)
    behind = jnp.einsum("ji,njh->nih", lower, parts[:, :, 1], precision=lax.Precision.HIGHEST)
    return jnp.stack([ahead, behind], axis=2).reshape(log_decay.shape)


def body(
    latent,
    context,
    condition,
    context_condition,
    shift_weight,
    scale_weight,
    gate_weight,
    norm_gain,
    query_weight,
    key_weight,
    value_weight,
    write_weight,
    decay_weight,
    write_bias,
    decay_bias,
    log_rate,
    head_gain,
    out_weight,
):
    heads_here = query_weight.shape[1] // HEAD_DIM
    first_head = lax.axis_index("tp") * heads_here
    tokens, ctx_tokens = latent.shape[0], context.shape[0]
    stacked = jnp.stack([condition, context_condition]).astype(f32)
    silu_rows = jax.nn.silu(stacked).astype(bf16)
    rows, gate_row = modulation(silu_rows, shift_weight, scale_weight, gate_weight)

    def modulate(row_data, row_index):
        normed = rms_rows(row_data, norm_gain)
        return (normed * (1.0 + rows[2 + row_index]) + rows[row_index]).astype(bf16)

    modulated = jnp.concatenate([modulate(latent, 0), modulate(context, 1)], axis=0)

    def own_heads(array):
        return lax.dynamic_slice_in_dim(array, first_head, heads_here, array.ndim - 1)

    gate_weights = jnp.concatenate(
        [
            own_heads(write_weight).reshape(write_weight.shape[0], -1),
            own_heads(decay_weight).reshape(decay_weight.shape[0], -1),
        ],
        axis=1,
    )
    queries = project(modulated, query_weight)
    keys = project(modulated, key_weight)
    values = project(modulated, value_weight)
    pre = project(modulated, gate_weights).astype(f32).reshape(-1, 2, 2, heads_here)
    rate = jax.nn.sigmoid(pre[:, 0] + own_heads(write_bias))
    log_decay = -jnp.exp(own_heads(log_rate)) * jax.nn.softplus(pre[:, 1] + own_heads(decay_bias))
    lat, ctx = spans(tokens, ctx_tokens)
    running = jnp.concatenate(
        [running_sums(log_decay[:tokens], lat[0][1]), running_sums(log_decay[tokens:], ctx[0][1])], axis=0
    )
    gates = jnp.stack([rate, running], axis=2)
    col = jnp.transpose(gates, (3, 0, 1, 2)).reshape(heads_here, tokens + ctx_tokens, 4)
    row = jnp.transpose(gates, (3, 1, 2, 0)).reshape(heads_here, 4, tokens + ctx_tokens)
    head_out = exchange(queries, keys, values, col, row, head_gain[None, :], tokens, ctx_tokens)
    return output(head_out, gate_row, latent, out_weight)


def solution(mesh):
    placed = (
        P("sp", None),
        P("sp", None),
        P("sp"),
        P("sp"),
        P("sp", "tp"),
        P("sp", "tp"),
        P("sp", "tp"),
        P(),
        P(None, "tp"),
        P(None, "tp"),
        P(None, "tp"),
        P(),
        P(),
        P(),
        P(),
        P(),
        P(),
        P(None, "tp"),
    )
    return jax.shard_map(body, mesh=mesh, in_specs=placed, out_specs=P("sp", "tp"), check_vma=False)
```

profile of v0, /device:TPU:1, one launch (start us, length us, event | category | flops | bytes accessed | tf_op | source)
XLA Modules:
  0.0 113.1 jit_solution(9709929890768630536)
XLA Ops:
  0.0 0.0 copy-start.5
  0.0 0.0 copy-start.4
  0.0 0.0 copy-start.6
  0.0 0.0 copy-start.7
  0.0 1.3 %fusion.6 = f32[64]{0:T(128)S(1)} fusion(bf16[64,4096]{1,0:T(8,128)(2,1)} %param.19), kind=kLoop, calls=%fused_computation.19 | loop fusion | flops 786368 | bytes 524544 | tf_op jit(solution)/shard_map/reduce_sum | solution.py:489
  1.3 0.7 stack.34
  2.0 0.7 stack.35
  2.7 0.8 fusion.39
  3.4 3.1 %fusion = f32[512]{0:T(512)S(1)} fusion(bf16[512,4096]{1,0:T(8,128)(2,1)} %latent_ref.1), kind=kLoop, calls=%fused_computation.2 | loop fusion | flops 6290944 | bytes 4196352 | tf_op jit(solution)/shard_map/reduce_sum | solution.py:489
  6.5 0.0 copy-done.6
  6.6 0.0 copy-done.7
  6.6 0.1 constant_dynamic-slice_fusion
  6.6 0.6 pad.4.silu_ref
  7.2 19.8 %modulation.1 = (f32[4,4096]{1,0:T(4,128)}, f32[1,512]{1,0:T(1,128)}) custom-call(bf16[8,256]{1,0:T(8,128)(2,1)} %pad.4.silu_ref, bf16[256,512]{1,0:T(8,128)(2,1)} %shift_ref.1, bf16[256,512]{1,0:T(8,128)(2,1)} %scale_ref.1, bf16[256,512]{1,0:T(8,128)(2,1)} %gate_ref.1), custom_call_target="tpu_custom_call" | custom-call | tf_op jit(solution)/shard_map/modulation/pallas_call | solution.py:212
  27.1 1.1 %slice_add_fusion.1 = (f32[1,4096]{1,0:T(1,128)S(1)}, f32[1,4096]{1,0:T(1,128)S(1)}, f32[1,4096]{1,0:T(1,128)S(1)}, f32[1,4096]{1,0:T(1,128)S(1)}) fusion(f32[4,4096]{1,0:T(4,128)} %get-tuple-element.7), kind=kLoop, calls=%fused_computation.46 | loop fusion | flops 8192 | bytes 131072 | tf_op jit(solution)/shard_map/add | solution.py:534
  28.2 1.0 constant_dynamic-slice_fusion.3
  29.3 0.0 copy-done.5
  29.3 0.0 copy-done.4
  29.3 0.3 fusion.10
  29.6 4.1 %fusion.4 = bf16[512,4096]{1,0:T(8,128)(2,1)S(1)} fusion(bf16[512,4096]{1,0:T(8,128)(2,1)} %latent_ref.1, f32[4096]{0:T(1024)S(1)} %bitcast.87, f32[4096]{0:T(1024)S(1)} %bitcast.86, f32[4096]{0:T(1024)S(1)} %copy-done.5, f32[512]{0:T(512)S(1)} %add_rsqrt_fusion), kind=kLoop, calls=%fused_computation.6 | loop fusion | flops 12582912 | bytes 8439808 | tf_op jit(solution)/shard_map/convert_element_type | solution.py:534
  33.7 0.0 copy-start.2
  33.7 1.9 %copy-done.2 = bf16[512,4096]{1,0:T(8,128)(2,1)} copy-done((bf16[512,4096]{1,0:T(8,128)(2,1)}, bf16[512,4096]{1,0:T(8,128)(2,1)S(1)}, u32[]{:S(2)}) %copy-start.2) | copy-done | bytes 4194328
  35.6 1.3 %fusion.5 = f32[576,8]{0,1:T(8,128)S(1)} fusion(bf16[4096,4]{0,1:T(4,128)(2,1)S(1)} %reshape.85, bf16[4096,4]{0,1:T(4,128)(2,1)S(1)} %reshape.84, bf16[64,4096]{1,0:T(8,128)(2,1)S(1)} %fusion.10, bf16[512,4096]{1,0:T(8,128)(2,1)S(1)} %fusion.4), kind=kOutput, calls=%fused_computation.14 | convolution fusion | flops 47326208 | bytes 4802560 | tf_op jit(solution)/shard_map/dot_general | solution.py:494
  37.0 0.1 fusion.28
  37.1 0.1 fusion.34
  37.2 0.1 convolution_bitcast_fusion.2
  37.3 0.2 convolution_bitcast_fusion.3
  37.5 0.2 convolution_bitcast_fusion
  37.7 0.2 convolution_bitcast_fusion.1
  38.0 0.0 copy-start.3
  38.0 0.0 copy-start.8
  38.0 4.4 %convolution_convert_fusion.1.k_ref = bf16[576,256]{1,0:T(8,128)(2,1)S(1)} fusion(bf16[4096,256]{1,0:T(8,128)(2,1)} %param.27, bf16[64,4096]{1,0:T(8,128)(2,1)S(1)} %fusion.10, bf16[512,4096]{1,0:T(8,128)(2,1)} %copy-done.2), kind=kOutput, calls=%fused_computation.11 | convolution fusion | flops 1217544192 | bytes 7110656 | tf_op jit(solution)/shard_map/dot_general | solution.py:494
  42.4 0.0 copy-done.3
  42.4 0.3 copy-done.8
  42.8 0.0 copy-start.9
  42.8 1.4 %convolution_convert_fusion.v_ref = bf16[576,256]{1,0:T(8,128)(2,1)S(1)} fusion(bf16[4096,256]{1,0:T(8,128)(2,1)S(1)} %copy-done.8, bf16[64,4096]{1,0:T(8,128)(2,1)S(1)} %fusion.10, bf16[512,4096]{1,0:T(8,128)(2,1)S(1)} %copy-done.3), kind=kOutput, calls=%fused_computation.10 | convolution fusion | flops 1217544192 | bytes 7110656 | tf_op jit(solution)/shard_map/dot_general | solution.py:494
  44.1 0.2 copy-done.9
  44.3 0.0 copy-start.1
  44.3 1.4 %convolution_convert_fusion.2.q_ref = bf16[576,256]{1,0:T(8,128)(2,1)S(1)} fusion(bf16[4096,256]{1,0:T(8,128)(2,1)S(1)} %copy-done.9, bf16[64,4096]{1,0:T(8,128)(2,1)S(1)} %fusion.10, bf16[512,4096]{1,0:T(8,128)(2,1)S(1)} %copy-done.3), kind=kOutput, calls=%fused_computation.12 | convolution fusion | flops 1217544192 | bytes 7110656 | tf_op jit(solution)/shard_map/dot_general | solution.py:494
  45.7 0.2 copy.22.col_ref
  46.0 0.0 copy-done.1
  46.0 44.6 %exchange.1.head_ref = bf16[512,256]{1,0:T(8,128)(2,1)S(1)} custom-call(bf16[576,256]{1,0:T(8,128)(2,1)S(1)} %convolution_convert_fusion.2.q_ref, bf16[576,256]{1,0:T(8,128)(2,1)S(1)} %convolution_convert_fusion.1.k_ref, bf16[576,256]{1,0:T(8,128)(2,1)S(1)} %convolution_convert_fusion.v_ref, f32[2,576,4]{2,1,0:T(8,128)S(1)} %copy.22.col_ref, ...), custom_call_target="tpu_custom_call" | custom-call | tf_op jit(solution)/shard_map/exchange/pallas_call | solution.py:359
  90.6 0.0 copy-start
  90.6 0.7 copy-done
  91.3 19.9 %output.1 = bf16[512,512]{1,0:T(8,128)(2,1)} custom-call(bf16[512,256]{1,0:T(8,128)(2,1)} %copy-done, f32[1,512]{1,0:T(1,128)} %get-tuple-element.8.gate_ref, bf16[512,4096]{1,0:T(8,128)(2,1)} %latent_ref.1, bf16[2048,512]{1,0:T(8,128)(2,1)} %weight_ref.1), custom_call_target="tpu_custom_call" | custom-call | tf_op jit(solution)/shard_map/output/pallas_call | solution.py:462
  111.2 1.9 %copy.25 = bf16[512,512]{1,0:T(8,128)(2,1)} copy(bf16[512,512]{1,0:T(8,128)(2,1)} %output.1) | data formatting | bytes 1048576
  (15 shorter events, 0.2 us)
Async XLA Ops:
  0.0 29.3 %copy-start.5 = (f32[4096]{0:T(1024)S(1)}, f32[4096]{0:T(1024)}, u32[]{:S(2)}) copy-start(f32[4096]{0:T(1024)} %param.25) | copy-start | bytes 49156
  0.0 29.3 %copy-start.4 = (bf16[64,4096]{1,0:T(8,128)(2,1)S(1)}, bf16[64,4096]{1,0:T(8,128)(2,1)}, u32[]{:S(2)}) copy-start(bf16[64,4096]{1,0:T(8,128)(2,1)} %param.19) | copy-start | bytes 1572868
  0.0 6.5 %copy-start.6 = (f32[2,16]{1,0:T(2,128)S(1)}, f32[2,16]{1,0:T(2,128)}, u32[]{:S(2)}) copy-start(f32[2,16]{1,0:T(2,128)} %param.32) | copy-start | bytes 388
  0.0 6.5 %copy-start.7 = (f32[2,16]{1,0:T(2,128)S(1)}, f32[2,16]{1,0:T(2,128)}, u32[]{:S(2)}) copy-start(f32[2,16]{1,0:T(2,128)} %param.31) | copy-start | bytes 388
  33.7 1.9 %copy-start.2 = (bf16[512,4096]{1,0:T(8,128)(2,1)}, bf16[512,4096]{1,0:T(8,128)(2,1)S(1)}, u32[]{:S(2)}) copy-start(bf16[512,4096]{1,0:T(8,128)(2,1)S(1)} %fusion.4) | copy-start | bytes 12582916
  38.0 4.4 %copy-start.3 = (bf16[512,4096]{1,0:T(8,128)(2,1)S(1)}, bf16[512,4096]{1,0:T(8,128)(2,1)}, u32[]{:S(2)}) copy-start(bf16[512,4096]{1,0:T(8,128)(2,1)} %copy-done.2) | copy-start | bytes 12582916
  38.0 4.7 %copy-start.8 = (bf16[4096,256]{1,0:T(8,128)(2,1)S(1)}, bf16[4096,256]{1,0:T(8,128)(2,1)}, u32[]{:S(2)}) copy-start(bf16[4096,256]{1,0:T(8,128)(2,1)} %param.28) | copy-start | bytes 6291460
  42.8 1.6 %copy-start.9 = (bf16[4096,256]{1,0:T(8,128)(2,1)S(1)}, bf16[4096,256]{1,0:T(8,128)(2,1)}, u32[]{:S(2)}) copy-start(bf16[4096,256]{1,0:T(8,128)(2,1)} %param.26) | copy-start | bytes 6291460
  44.3 1.6 %copy-start.1 = (f32[128]{0:T(128)S(1)}, f32[128]{0:T(128)}, u32[]{:S(2)}) copy-start(f32[128]{0:T(128)} %param.34) | copy-start | bytes 1540
  90.6 0.7 copy-start
where the time goes:
time: 114 us; the launch traced here: 113 us
  Pallas kernels  84.3 us (74%)
  other arithmetic  10.9 us (10%)
  matrix products  9.15 us (8%)
  local copies, waits for them, and re-layouts  8.46 us (7%)
    pallas_call x1, Pallas kernels, exchange(): pl.pallas_call(functools.partial(exchange_kernel, sp, per, tokens, ctx_to...  44.6 us
    pallas_call x1, Pallas kernels, output(): pl.pallas_call(functools.partial(output_kernel, tp, pieces), in_specs=[vm...  19.9 us
    pallas_call x1, Pallas kernels, modulation(): pl.pallas_call(functools.partial(modulation_kernel, sp, tp), in_specs=[vm...  19.8 us
    dot_general x4, matrix products, project(): return jnp.dot(matrix, weight, preferred_element_type=f32).astype(bf16)  8.46 us
    unnamed x21, local copies, waits for them, and re-layouts  5.04 us
    reduce_sum x2, other arithmetic, rms_rows(): jnp.mean(values * values, axis=-1, keepdims=True) + epsilon  4.39 us
    convert_element_type x2, other arithmetic, modulate(): return (normed * (1.0 + rows[2 + row_index]) + rows[row_index]).astype(bf16)  4.33 us

commit v1 on v0

v1 whole, which is shorter than its diff:
```python
import functools

import jax
import jax.numpy as jnp
from jax import lax
from jax.experimental import pallas as pl
from jax.experimental.pallas import tpu as pltpu
from jax.sharding import PartitionSpec as P

HEAD_DIM = 128
CHUNK = 128
epsilon = 0.0001
bf16 = jnp.bfloat16
f32 = jnp.float32


def mm(a, b):
    return jnp.dot(a.astype(bf16), b.astype(bf16), preferred_element_type=f32)


def mm_t(a, b):
    return lax.dot_general(a, b, (((1,), (1,)), ((), ())), preferred_element_type=f32)


def spans(tokens, ctx_tokens):
    size = min(CHUNK, tokens)
    lat = [(at, size) for at in range(0, tokens, size)]
    ctx_size = min(CHUNK, ctx_tokens)
    ctx = [(tokens + at, ctx_size) for at in range(0, ctx_tokens, ctx_size)]
    return lat, ctx


def iotas(size):
    rows = lax.broadcasted_iota(jnp.int32, (size, size), 0)
    cols = lax.broadcasted_iota(jnp.int32, (size, size), 1)
    return rows, cols


def prepare(groups):
    items = []
    for group in groups:
        size = group["size"]
        rows, cols = iotas(size)
        keys = group["k"]
        keys_t = keys.astype(f32).T
        gram = jnp.dot(keys, keys_t.astype(bf16), preferred_element_type=f32)
        diag = jnp.where(rows == cols, gram, 0.0)
        s_col = lax.rsqrt(jnp.sum(diag, axis=1, keepdims=True) + epsilon)
        s_row = lax.rsqrt(jnp.sum(diag, axis=0, keepdims=True) + epsilon)
        gram = gram * s_col * s_row
        group["keys"] = keys.astype(f32) * s_col
        group["keys_t"] = keys_t * s_row
        group["values"] = group["v"].astype(f32)
        if group["q"] is not None:
            queries = group["q"].astype(f32)
            q_scale = lax.rsqrt(jnp.sum(queries * queries, axis=1, keepdims=True) + epsilon) * HEAD_DIM**-0.5
            group["queries"] = queries * q_scale
            group["score"] = (
                jnp.dot(group["q"], keys_t.astype(bf16), preferred_element_type=f32) * q_scale * s_row
            )
        for d in range(2):
            rate_col, run_col, run_row = group["gates"][d]
            inside = rows >= cols if d == 0 else rows <= cols
            strict = rows > cols if d == 0 else rows < cols
            decay = jnp.where(inside, jnp.exp(jnp.minimum(run_col - run_row, 0.0)), 0.0)
            system = jnp.where(strict, gram * decay * rate_col, 0.0)
            item = dict(group=group, size=size, d=d, rate_col=rate_col, run_col=run_col, run_row=run_row)
            item["system"] = system
            if group["q"] is not None:
                item["score"] = group["score"] * decay
            near = (rows // 2) == (cols // 2)
            item["inv"] = jnp.where(rows == cols, 1.0, jnp.where(near, -system, 0.0))
            items.append(item)
    span = 2
    while span < max(item["size"] for item in items):
        firsts = []
        for item in items:
            if span >= item["size"]:
                firsts.append(None)
                continue
            rows, cols = iotas(item["size"])
            rows, cols = rows // span, cols // span
            if item["d"] == 0:
                mask = ((rows % 2) == 1) & (cols == rows - 1)
            else:
                mask = ((cols % 2) == 1) & (rows == cols - 1)
            firsts.append(mm(jnp.where(mask, item["system"], 0.0), item["inv"]))
        for item, first in zip(items, firsts):
            if first is not None:
                item["inv"] = item["inv"] - mm(item["inv"], first)
        span *= 2
    for item in items:
        group = item["group"]
        growth = jnp.exp(item["run_col"])
        both = jnp.concatenate(
            [group["values"] * item["rate_col"], group["keys"] * (item["rate_col"] * growth)], axis=1
        )
        item["solved"] = mm(item["inv"], both)
        last = item["run_row"][:, item["size"] - 1 :] if item["d"] == 0 else item["run_row"][:, :1]
        item["gate"] = jnp.exp(last)
        late_t = group["keys_t"] * jnp.exp(last - item["run_row"])
        item["late"] = mm(late_t, item["solved"])
        if group["q"] is not None:
            weighed = mm(item["score"], item["solved"])
            item["local"] = weighed[:, :HEAD_DIM]
            item["early"] = group["queries"] * growth - weighed[:, HEAD_DIM:]
    return items


def chain(items, d, e_ref):
    rows, cols = iotas(HEAD_DIM)
    eye = (rows == cols).astype(f32)
    carry = None
    for item in items if d == 0 else items[::-1]:
        if e_ref is not None:
            if carry is None:
                out, early = item["local"], item["early"]
            else:
                moved = mm(item["early"], carry)
                out = item["local"] + moved[:, :HEAD_DIM]
                early = item["early"] + moved[:, HEAD_DIM:]
            at, size = item["group"]["at"], item["size"]
            e_ref[at : at + size, d * HEAD_DIM : (d + 1) * HEAD_DIM] = early.astype(bf16)
            item["out"] = out
        late, gate = item["late"], item["gate"]
        fresh = jnp.concatenate([late[:, :HEAD_DIM], (gate - 1.0) * eye - late[:, HEAD_DIM:]], axis=1)
        if carry is None:
            carry = fresh
        else:
            carry = gate * carry + fresh - mm(late[:, HEAD_DIM:], carry)
    return carry


def on_mesh(sp=None, tp=None):
    return (lax.axis_index("sp") if sp is None else sp, lax.axis_index("tp") if tp is None else tp)


def send(src, dst, send_sem, recv_sem, device):
    return pltpu.make_async_remote_copy(
        src_ref=src,
        dst_ref=dst,
        send_sem=send_sem,
        recv_sem=recv_sem,
        device_id=device,
        device_id_type=pl.DeviceIdType.MESH,
    )


def greet(devices):
    barrier = pltpu.get_barrier_semaphore()
    for device in devices:
        pl.semaphore_signal(barrier, inc=1, device_id=device, device_id_type=pl.DeviceIdType.MESH)


def split_three(x):
    high = x.astype(bf16)
    rest = x - high.astype(f32)
    mid = rest.astype(bf16)
    low = (rest - mid.astype(f32)).astype(bf16)
    return jnp.concatenate([high, mid, low], axis=1)


def advance(state, move, add):
    high = state.astype(bf16)
    low = (state - high.astype(f32)).astype(bf16)
    both = jnp.concatenate([high, low], axis=0)
    moved = jnp.dot(both, move, preferred_element_type=f32)
    rows = state.shape[0]
    return state + add.astype(f32) + moved[:rows] + moved[rows:]


def mixer_kernel(
    sp, tp, heads, tokens, ctx_tokens,
    cond_ref, ctx_cond_ref, gain_ref, head_gain_ref, write_bias_ref, decay_bias_ref, log_rate_ref,
    latent_hbm, context_hbm, shift_hbm, scale_hbm, gate_hbm, query_hbm, key_hbm, value_hbm,
    write_hbm, decay_hbm, out_hbm,
    out_ref,
    rows_v, mod_w, q_w, k_w, v_w, gate_w, out_w, st, stats, mod_v, q_v, k_v, v_v, rate_v, run_v, run_t,
    got_p, blocks, gate_row, o_v, e_v, maps_m, maps_b, got_m, got_b, starts, back, got_o, acc,
    load, sent_p, recv_p, sent_t, recv_t, sent_m, recv_m, sent_b, recv_b, sent_s, recv_s,
    sent_up, recv_dn, sent_dn, recv_up, sent_f, recv_f, sent_c, recv_c,
):
    me, col = lax.axis_index("sp"), lax.axis_index("tp")
    items = 2 * heads
    split = sp // items
    part_rows = HEAD_DIM // split
    half_owners = sp // heads
    width = mod_w.shape[2]
    half = width // 2
    total_tokens = tokens + ctx_tokens
    rings = [lax.rem(me + r, sp) for r in range(1, sp)]
    cross = [lax.rem(col + r, tp) for r in range(1, tp)]
    greet([on_mesh(sp=place) for place in rings] + [on_mesh(tp=place) for place in cross])

    def fetch(n, src, dst):
        copy = pltpu.make_async_copy(src, dst, load.at[n])
        copy.start()
        return copy

    gates_rows = write_hbm.shape[0]
    mod_loads = [fetch(n, src, mod_w.at[n]) for n, src in enumerate((shift_hbm, scale_hbm, gate_hbm))]
    row_loads = [
        fetch(3, latent_hbm, rows_v.at[pl.ds(0, tokens)]),
        fetch(4, context_hbm, rows_v.at[pl.ds(tokens, ctx_tokens)]),
    ]
    weight_loads = [
        fetch(5, key_hbm, k_w),
        fetch(6, value_hbm, v_w),
        fetch(7, write_hbm, gate_w.at[pl.ds(0, gates_rows)]),
        fetch(8, decay_hbm, gate_w.at[pl.ds(gates_rows, gates_rows)]),
        fetch(9, query_hbm, q_w),
    ]
    out_load = fetch(10, out_hbm, out_w)

    def silu(ref):
        value = ref[...].astype(f32)
        return value / (1.0 + jnp.exp(-value))

    silus = (silu(cond_ref), silu(ctx_cond_ref))
    quarter = silus[0].shape[0]
    lefts = []
    for part in range(quarter):
        lefts.append(
            jnp.concatenate(
                [silus[0][part : part + 1], silus[1][part : part + 1], jnp.zeros((6, silus[0].shape[1]), f32)], axis=0
            ).astype(bf16)
        )
    left = jnp.concatenate(lefts, axis=1)
    for copy in mod_loads:
        copy.wait()
    shift = jnp.dot(left, mod_w[0], preferred_element_type=f32)
    scale = jnp.dot(left, mod_w[1], preferred_element_type=f32)
    gate = jnp.dot(left, mod_w[2], preferred_element_type=f32)
    partial = jnp.concatenate([shift[0:2], scale[0:2], gate[0:1], jnp.zeros((3, width), f32)], axis=0)
    got_p[me] = jnp.concatenate([partial[:, :half], partial[:, half:]], axis=0).astype(bf16)
    pl.semaphore_wait(pltpu.get_barrier_semaphore(), len(rings) + len(cross))
    out = []
    for r, place in enumerate(rings):
        out.append(send(got_p.at[me], got_p.at[me], sent_p.at[r], recv_p.at[me], on_mesh(sp=place)))
        out[-1].start()

    gate_w[2 * gates_rows :, :] = jnp.zeros((gate_w.shape[0] - 2 * gates_rows, gate_w.shape[1]), bf16)
    for copy in row_loads:
        copy.wait()

    def measure_rows(i, unused):
        at = pl.ds(pl.multiple_of(i * 32, 32), 32)
        values = rows_v[at, :].astype(f32)
        mean = jnp.mean(values * values, axis=1, keepdims=True)
        stats[at, :] = jnp.broadcast_to(lax.rsqrt(mean + epsilon), (32, HEAD_DIM))
        return unused

    lax.fori_loop(0, total_tokens // 32, measure_rows, 0)

    for place in rings:
        spot = got_p.at[place]
        send(spot, spot, sent_p.at[0], recv_p.at[place], on_mesh(sp=place)).wait_recv()
    total = got_p[0].astype(f32)
    for place in range(1, sp):
        total = total + got_p[place].astype(f32)
    blocks[col] = jnp.concatenate([total[0:4], total[8:12]], axis=0)
    gate_row[...] = jnp.concatenate([total[4:5], total[12:13]], axis=1)
    for r, place in enumerate(cross):
        out.append(send(blocks.at[col], blocks.at[col], sent_t.at[r], recv_t.at[col], on_mesh(tp=place)))
        out[-1].start()
    for place in cross:
        spot = blocks.at[place]
        send(spot, spot, sent_t.at[0], recv_t.at[place], on_mesh(tp=place)).wait_recv()
    for place in range(tp):
        at = place * width
        for part in range(2):
            lanes = slice(at + part * half, at + (part + 1) * half)
            four = blocks[place, 4 * part : 4 * part + 4, :]
            st[0:2, lanes] = four[0:2]
            st[2:4, lanes] = (1.0 + four[2:4]) * gain_ref[:, lanes]

    def modulate(first, count, which):
        def step(i, unused):
            at = pl.ds(pl.multiple_of(first + i * 16, 16), 16)
            values = rows_v[at, :].astype(f32) * stats[at, 0:1]
            mod_v[at, :] = (values * st[2 + which : 3 + which, :] + st[which : which + 1, :]).astype(bf16)
            return unused

        lax.fori_loop(0, count // 16, step, 0)

    modulate(tokens, ctx_tokens, 1)
    modulate(0, tokens, 0)
    for copy in weight_loads:
        copy.wait()
    pre = mm_t(mod_v[...], gate_w[...]).astype(bf16).astype(f32)
    k_v[...] = jnp.dot(mod_v[...], k_w[...], preferred_element_type=f32).astype(bf16)
    v_v[...] = jnp.dot(mod_v[...], v_w[...], preferred_element_type=f32).astype(bf16)
    q_v[...] = jnp.dot(mod_v[0:tokens, :], q_w[...], preferred_element_type=f32).astype(bf16)

    all_heads = gates_rows // 2
    first_head = col * heads
    pre = pltpu.roll(pre, HEAD_DIM - first_head, 1)
    lane = lax.broadcasted_iota(jnp.int32, (1, HEAD_DIM), 1)
    write_bias = jnp.zeros((1, HEAD_DIM), f32)
    decay_bias = jnp.zeros((1, HEAD_DIM), f32)
    log_rate = jnp.zeros((1, HEAD_DIM), f32)
    for d in range(2):
        for head in range(heads):
            spot = d * all_heads + head
            write_bias = jnp.where(lane == spot, write_bias_ref[d, first_head + head], write_bias)
            decay_bias = jnp.where(lane == spot + gates_rows, decay_bias_ref[d, first_head + head], decay_bias)
            log_rate = jnp.where(lane == spot + gates_rows, log_rate_ref[d, first_head + head], log_rate)
    rate_v[...] = jax.nn.sigmoid(pre + write_bias)
    raised = pre + decay_bias
    soft = jnp.maximum(raised, 0.0) + jnp.log1p(jnp.exp(-jnp.abs(raised)))
    log_decay = -jnp.exp(log_rate) * soft
    lat, ctx = spans(tokens, ctx_tokens)
    for n, (at, size) in enumerate(lat + ctx):
        rows, cols = iotas(size)
        lower = (rows >= cols).astype(f32)
        upper = (rows <= cols).astype(f32)
        sums = jnp.dot(
            jnp.concatenate([lower, upper], axis=0).astype(bf16),
            split_three(log_decay[at : at + size]),
            preferred_element_type=f32,
        )
        sums = sums[:, :HEAD_DIM] + sums[:, HEAD_DIM : 2 * HEAD_DIM] + sums[:, 2 * HEAD_DIM :]
        running = jnp.where(lane < gates_rows + all_heads, sums[:size], sums[size:])
        run_v[at : at + size, :] = running
        run_t[n, :, :size] = running.T

    def group_of(n, at, size, head, latent):
        lanes = slice(head * HEAD_DIM, (head + 1) * HEAD_DIM)
        gates = []
        for d in range(2):
            spot = d * all_heads + head
            deep = spot + gates_rows
            gates.append(
                (
                    rate_v[at : at + size, spot : spot + 1],
                    run_v[at : at + size, deep : deep + 1],
                    run_t[n, deep : deep + 1, :size],
                )
            )
        return dict(
            at=at,
            size=size,
            k=k_v[at : at + size, lanes],
            v=v_v[at : at + size, lanes],
            q=q_v[at : at + size, lanes] if latent else None,
            gates=gates,
        )

    def keep(part, item, carry):
        maps_b[part, item] = carry[:, :HEAD_DIM].T.astype(bf16)
        maps_m[part, item] = carry[:, HEAD_DIM:].T.astype(bf16)

    my_item, my_part = me // split, lax.rem(me, split)

    def ship(part, owner):
        item, piece = owner // split, lax.rem(owner, split)
        return (
            send(
                maps_m.at[part, item], got_m.at[part, me], sent_m.at[part, owner], recv_m.at[part, me],
                on_mesh(sp=owner),
            ),
            send(
                maps_b.at[part, item, pl.ds(pl.multiple_of(piece * part_rows, part_rows), part_rows)],
                got_b.at[part, me], sent_b.at[part, owner], recv_b.at[part, me], on_mesh(sp=owner),
            ),
        )

    def ship_head(part, head):
        base = head * half_owners
        for r in range(1, half_owners):
            for copy in ship(part, base + lax.rem(me + r, half_owners)):
                copy.start()

        @pl.when(me // half_owners != head)
        def _():
            for copy in ship(part, base + lax.rem(me, half_owners)):
                copy.start()

    def keep_own(part):
        got_m[part, me] = maps_m[part, my_item]
        got_b[part, me] = maps_b[part, my_item, pl.ds(pl.multiple_of(my_part * part_rows, part_rows), part_rows), :]

    ctx_items = {}
    ctx_groups = []
    for head in range(heads):
        for n, (at, size) in enumerate(ctx):
            ctx_groups.append(group_of(len(lat) + n, at, size, head, False))
    done = prepare(ctx_groups)
    each = 2 * len(ctx)
    for head in range(heads):
        for d in range(2):
            chosen = [i for i in done[head * each : (head + 1) * each] if i["d"] == d]
            keep(0, 2 * head + d, chain(chosen, d, None))
    for head in range(heads):
        ship_head(0, head)
    for head in range(heads):
        done = prepare([group_of(n, at, size, head, True) for n, (at, size) in enumerate(lat)])
        for d in range(2):
            keep(1, 2 * head + d, chain([i for i in done if i["d"] == d], d, e_v.at[head]))
        for at, size in lat:
            pair = [i for i in done if i["group"]["at"] == at]
            o_v[head, at : at + size, :] = pair[0]["out"] + pair[1]["out"]
        ship_head(1, head)
    keep_own(0)
    keep_own(1)

    reverse = lax.rem(my_item, 2)

    def arrive(part):
        for place in rings:
            spot = got_m.at[part, place]
            send(spot, spot, sent_m.at[part, 0], recv_m.at[part, place], on_mesh(sp=place)).wait_recv()
            spot = got_b.at[part, place]
            send(spot, spot, sent_b.at[part, 0], recv_b.at[part, place], on_mesh(sp=place)).wait_recv()

    arrive(0)
    state = jnp.zeros((part_rows, HEAD_DIM), f32)
    for step in range(sp):
        place = step + reverse * (sp - 1 - 2 * step)
        state = advance(state, got_m[0, place], got_b[0, place])
    arrive(1)
    for step in range(sp):
        place = step + reverse * (sp - 1 - 2 * step)
        starts[place] = state.astype(bf16)
        if step < sp - 1:
            state = advance(state, got_m[1, place], got_b[1, place])
    back[me] = starts[me]

    def give_back(place):
        return send(starts.at[place], back.at[me], sent_s.at[place], recv_s.at[me], on_mesh(sp=place))

    for place in rings:
        give_back(place).start()

    core = lax.rem(col, 2)
    chips = tp // 2
    chip = col // 2
    partner = col + 1 - 2 * core
    up = lax.rem(chip + 1, chips) * 2 + core
    down = lax.rem(chip + chips - 1, chips) * 2 + core
    far = lax.rem(chip + 2, chips) * 2 + core
    mid = tokens // 2

    def piece(head, place, part):
        return got_o.at[head, place, pl.ds(part * mid, mid)]

    def to_up(head, part):
        return send(
            piece(head, col, part), piece(head, col, part), sent_up.at[head, part], recv_dn.at[head, part],
            on_mesh(tp=up),
        )

    def to_down(head, part):
        return send(
            piece(head, col, part), piece(head, col, part), sent_dn.at[head, part], recv_up.at[head, part],
            on_mesh(tp=down),
        )

    def forward(head, part):
        src, dst = (down, up) if part == 0 else (up, down)
        return send(
            piece(head, src, part), piece(head, src, part), sent_f.at[head, part], recv_f.at[head, part],
            on_mesh(tp=dst),
        )

    def relay(head, n, spot):
        return send(spot, spot, sent_c.at[head, n], recv_c.at[head, n], on_mesh(tp=partner))

    def finish_head(head):
        half_items = [2 * head, 2 * head + 1]
        for owner in range(2 * head * split, 2 * (head + 1) * split):

            @pl.when(owner != me)
            def _():
                spot = back.at[owner]
                send(spot, spot, sent_s.at[owner], recv_s.at[owner], on_mesh(sp=owner)).wait_recv()

        pair = [back[item * split : (item + 1) * split].reshape(HEAD_DIM, HEAD_DIM) for item in half_items]
        combined = o_v[head] + mm_t(e_v[head], jnp.concatenate(pair, axis=1))
        norm = lax.rsqrt(jnp.mean(combined * combined, axis=1, keepdims=True) + epsilon)
        got_o[head, col] = (combined * norm * head_gain_ref[...]).astype(bf16)
        for copy in (to_up(head, 0), to_down(head, 1), to_up(head, 1), to_down(head, 0)):
            out.append(copy)
            copy.start()
        out.append(relay(head, 0, got_o.at[head, col]))
        out[-1].start()

    def near_arrivals(head):
        waits = ((down, 0, recv_dn, True), (up, 1, recv_up, True), (down, 1, recv_dn, False), (up, 0, recv_up, False))
        for n, (place, part, sems, onward) in enumerate(waits):
            spot = piece(head, place, part)
            send(spot, spot, sent_up.at[head, part], sems.at[head, part], on_mesh(tp=place)).wait_recv()
            if onward:
                out.append(forward(head, part))
                out[-1].start()
            out.append(relay(head, 1 + n, spot))
            out[-1].start()

    def far_arrivals(head):
        for part in range(2):
            spot = piece(head, far, part)
            send(spot, spot, sent_f.at[head, part], recv_f.at[head, part], on_mesh(tp=up)).wait_recv()
            out.append(relay(head, 5 + part, spot))
            out[-1].start()

    def from_partner(head, n, spot):
        send(spot, spot, sent_c.at[head, n], recv_c.at[head, n], on_mesh(tp=partner)).wait_recv()

    def add(head, place, first=False):
        even = place - core
        lanes = jnp.concatenate([got_o[head, even], got_o[head, even + 1]], axis=1)
        depth = heads * HEAD_DIM
        weights = jnp.concatenate(
            [
                out_w[pl.ds(pl.multiple_of((even + n) * depth + head * HEAD_DIM, HEAD_DIM), HEAD_DIM), :]
                for n in range(2)
            ],
            axis=0,
        )
        part = jnp.dot(lanes, weights, preferred_element_type=f32)
        acc[...] = part if first else acc[...] + part

    def near_matmuls(head):
        from_partner(head, 0, got_o.at[head, partner])
        add(head, col, head == 0)
        other = 1 - 2 * core
        for n, (place, part) in enumerate(((down, 0), (up, 1), (down, 1), (up, 0))):
            from_partner(head, 1 + n, piece(head, place + other, part))
        add(head, down)
        add(head, up)

    def far_matmuls(head):
        other = 1 - 2 * core
        for part in range(2):
            from_partner(head, 5 + part, piece(head, far + other, part))
        add(head, far)

    out_load.wait()
    finish_head(0)
    near_arrivals(0)
    for head in range(1, heads):
        finish_head(head)
        far_arrivals(head - 1)
        near_matmuls(head - 1)
        far_matmuls(head - 1)
        near_arrivals(head)
    far_arrivals(heads - 1)
    near_matmuls(heads - 1)
    far_matmuls(heads - 1)
    lanes = pl.ds(pl.multiple_of(col * width, width), width)
    out_ref[...] = rows_v[0:tokens, lanes].astype(f32) + gate_row[...] * acc[...]
    for copy in out:
        copy.wait_send()
    for part in range(2):
        for r in range(1, sp):
            for copy in ship(part, lax.rem(me + r, sp)):
                copy.wait_send()
    for place in rings:
        give_back(place).wait_send()


def body(
    latent,
    context,
    condition,
    context_condition,
    shift_weight,
    scale_weight,
    gate_weight,
    norm_gain,
    query_weight,
    key_weight,
    value_weight,
    write_weight,
    decay_weight,
    write_bias,
    decay_bias,
    log_rate,
    head_gain,
    out_weight,
):
    sp, tp = lax.axis_size("sp"), lax.axis_size("tp")
    inner = query_weight.shape[1]
    heads = inner // HEAD_DIM
    tokens, ctx_tokens = latent.shape[0], context.shape[0]
    total = tokens + ctx_tokens
    features = latent.shape[1]
    width = shift_weight.shape[1]
    items = 2 * heads
    split = sp // items
    rows = HEAD_DIM // split
    chunks = sum(len(part) for part in spans(tokens, ctx_tokens))
    vmem = pl.BlockSpec(memory_space=pltpu.VMEM)
    smem = pl.BlockSpec(memory_space=pltpu.SMEM)
    anywhere = pl.BlockSpec(memory_space=pl.ANY)
    dma = pltpu.SemaphoreType.DMA
    flat = [jnp.transpose(w, (1, 2, 0)).reshape(-1, features) for w in (write_weight, decay_weight)]
    updated = pl.pallas_call(
        functools.partial(mixer_kernel, sp, tp, heads, tokens, ctx_tokens),
        in_specs=[vmem] * 4 + [smem] * 3 + [anywhere] * 11,
        out_specs=vmem,
        out_shape=jax.ShapeDtypeStruct((tokens, width), f32),
        scratch_shapes=[
            pltpu.VMEM((total, features), bf16),
            pltpu.VMEM((3,) + shift_weight.shape, bf16),
            pltpu.VMEM(query_weight.shape, bf16),
            pltpu.VMEM(key_weight.shape, bf16),
            pltpu.VMEM(value_weight.shape, bf16),
            pltpu.VMEM((HEAD_DIM, features), bf16),
            pltpu.VMEM(out_weight.shape, bf16),
            pltpu.VMEM((4, features), f32),
            pltpu.VMEM((total, HEAD_DIM), f32),
            pltpu.VMEM((total, features), bf16),
            pltpu.VMEM((tokens, inner), bf16),
            pltpu.VMEM((total, inner), bf16),
            pltpu.VMEM((total, inner), bf16),
            pltpu.VMEM((total, HEAD_DIM), f32),
            pltpu.VMEM((total, HEAD_DIM), f32),
            pltpu.VMEM((chunks, HEAD_DIM, CHUNK), f32),
            pltpu.VMEM((sp, 16, width // 2), bf16),
            pltpu.VMEM((tp, 8, width // 2), f32),
            pltpu.VMEM((1, width), f32),
            pltpu.VMEM((heads, tokens, HEAD_DIM), f32),
            pltpu.VMEM((heads, tokens, 2 * HEAD_DIM), bf16),
            pltpu.VMEM((2, items, HEAD_DIM, HEAD_DIM), bf16),
            pltpu.VMEM((2, items, HEAD_DIM, HEAD_DIM), bf16),
            pltpu.VMEM((2, sp, HEAD_DIM, HEAD_DIM), bf16),
            pltpu.VMEM((2, sp, rows, HEAD_DIM), bf16),
            pltpu.VMEM((sp, rows, HEAD_DIM), bf16),
            pltpu.VMEM((sp, rows, HEAD_DIM), bf16),
            pltpu.VMEM((heads, tp, tokens, HEAD_DIM), bf16),
            pltpu.VMEM((tokens, width), f32),
            dma((11,)),
            dma((sp,)),
            dma((sp,)),
            dma((tp,)),
            dma((tp,)),
            dma((2, sp)),
            dma((2, sp)),
            dma((2, sp)),
            dma((2, sp)),
            dma((sp,)),
            dma((sp,)),
            dma((heads, 2)),
            dma((heads, 2)),
            dma((heads, 2)),
            dma((heads, 2)),
            dma((heads, 2)),
            dma((heads, 2)),
            dma((heads, 7)),
            dma((heads, 7)),
        ],
        compiler_params=pltpu.CompilerParams(
            collective_id=0, has_side_effects=True, vmem_limit_bytes=56 * 1024 * 1024
        ),
        name="mixer",
    )(
        condition.reshape(-1, HEAD_DIM),
        context_condition.reshape(-1, HEAD_DIM),
        norm_gain[None, :],
        head_gain[None, :],
        write_bias,
        decay_bias,
        log_rate,
        latent,
        context,
        shift_weight,
        scale_weight,
        gate_weight,
        query_weight,
        key_weight,
        value_weight,
        flat[0],
        flat[1],
        out_weight,
    )
    return updated.astype(bf16)


def solution(mesh):
    placed = (
        P("sp", None),
        P("sp", None),
        P("sp"),
        P("sp"),
        P("sp", "tp"),
        P("sp", "tp"),
        P("sp", "tp"),
        P(),
        P(None, "tp"),
        P(None, "tp"),
        P(None, "tp"),
        P(),
        P(),
        P(),
        P(),
        P(),
        P(),
        P(None, "tp"),
    )
    return jax.shard_map(body, mesh=mesh, in_specs=placed, out_specs=P("sp", "tp"), check_vma=False)
```

time: 114 us -> 75.1 us (0.66)
  Pallas kernels: 84.3 us -> 72.8 us
  matrix products: 9.15 us -> 0 us
  other arithmetic: 10.9 us -> 2.08 us
  local copies, waits for them, and re-layouts: 8.46 us -> 0 us
    pallas_call x3 -> x1, Pallas kernels: 84.3 us -> 72.8 us  [body(): pl.pallas_call(functools.partial(mixer_kernel, sp, tp, heads, tokens, ctx...]
    dot_general x8 -> x0, matrix products: 9.15 us -> none  [the longest x4 8.46 us: project(): return jnp.dot(matrix, weight, preferred_element_type=f32).astype(bf16)]
    unnamed x21 -> x0, local copies, waits for them, and re-layouts: 5.04 us -> none
    reduce_sum x2 -> x0, other arithmetic: 4.39 us -> none  [rms_rows(): jnp.mean(values * values, axis=-1, keepdims=True) + epsilon]
    convert_element_type x3 -> x1, other arithmetic: 4.35 us -> 2.08 us  [body(): return updated.astype(bf16)]
    another operation x4 -> x0, local copies, waits for them, and re-layouts: 1.36 us -> none  [the longest x2 1.33 us: body(): stacked = jnp.stack([condition, context_condition]).astype(f32)]
where the time goes in v1:
time: 75.1 us; the launch traced here: 74.9 us
  Pallas kernels  72.8 us (97%)
  other arithmetic  2.08 us (3%)
    pallas_call x1, Pallas kernels, body(): pl.pallas_call(functools.partial(mixer_kernel, sp, tp, heads, tokens, ctx...  72.8 us
    convert_element_type x1, other arithmetic, body(): return updated.astype(bf16)  2.08 us

profile of v1, /device:TPU:1, one launch (start us, length us, event | category | flops | bytes accessed | tf_op | source)
XLA Modules:
  0.0 74.9 jit_solution(11438048421177091801)
XLA Ops:
  0.0 72.8 %mixer.1 = f32[512,512]{1,0:T(8,128)} custom-call(bf16[2,128]{1,0:T(2,128)(2,1)} %bitcast.13, bf16[2,128]{1,0:T(2,128)(2,1)} %bitcast.14, f32[1,4096]{1,0:T(1,128)} %bitcast.12, f32[1,128]{1,0:T(1,128)} %bitcast.15, f32[2,16]{1,0:T(2,128)} %write_bias_ref.1, f32[2,16]{1,0:T(2,128)} %decay_bias_ref.1, f32[2,16]{1,0:T(2,128)} %log_rate_ref.1, ...), custom_call_target="tpu_custom_call" | custom-call | tf_op jit(solution)/shard_map/mixer/pallas_call | solution.py:598
  72.8 2.1 %convert_element_type.3 = bf16[512,512]{1,0:T(8,128)(2,1)} convert(f32[512,512]{1,0:T(8,128)} %mixer.1) | non-fusion elementwise | flops 262144 | bytes 1572864 | tf_op jit(solution)/shard_map/convert_element_type | solution.py:677

commit v2 on v1

--- a/solution.py
+++ b/solution.py
@@ -178,7 +178,7 @@
     rows_v, mod_w, q_w, k_w, v_w, gate_w, out_w, st, stats, mod_v, q_v, k_v, v_v, rate_v, run_v, run_t,
     got_p, blocks, gate_row, o_v, e_v, maps_m, maps_b, got_m, got_b, starts, back, got_o, acc,
     load, sent_p, recv_p, sent_t, recv_t, sent_m, recv_m, sent_b, recv_b, sent_s, recv_s,
-    sent_up, recv_dn, sent_dn, recv_up, sent_f, recv_f, sent_c, recv_c,
+    sent_o, recv_dn, recv_up, recv_f, recv_c,
 ):
     me, col = lax.axis_index("sp"), lax.axis_index("tp")
     items = 2 * heads
@@ -189,8 +189,15 @@
     half = width // 2
     total_tokens = tokens + ctx_tokens
     rings = [lax.rem(me + r, sp) for r in range(1, sp)]
+    near = on_mesh(sp=rings[0])
     cross = [lax.rem(col + r, tp) for r in range(1, tp)]
     greet([on_mesh(sp=place) for place in rings] + [on_mesh(tp=place) for place in cross])
+
+    def arrived(spot, sem):
+        send(spot, spot, sem, sem, near).wait_recv()
+
+    def left(spot, sem):
+        send(spot, spot, sem, sem, near).wait_send()
 
     def fetch(n, src, dst):
         copy = pltpu.make_async_copy(src, dst, load.at[n])
@@ -225,19 +232,17 @@
                 [silus[0][part : part + 1], silus[1][part : part + 1], jnp.zeros((6, silus[0].shape[1]), f32)], axis=0
             ).astype(bf16)
         )
-    left = jnp.concatenate(lefts, axis=1)
+    silu_rows = jnp.concatenate(lefts, axis=1)
     for copy in mod_loads:
         copy.wait()
-    shift = jnp.dot(left, mod_w[0], preferred_element_type=f32)
-    scale = jnp.dot(left, mod_w[1], preferred_element_type=f32)
-    gate = jnp.dot(left, mod_w[2], preferred_element_type=f32)
+    shift = jnp.dot(silu_rows, mod_w[0], preferred_element_type=f32)
+    scale = jnp.dot(silu_rows, mod_w[1], preferred_element_type=f32)
+    gate = jnp.dot(silu_rows, mod_w[2], preferred_element_type=f32)
     partial = jnp.concatenate([shift[0:2], scale[0:2], gate[0:1], jnp.zeros((3, width), f32)], axis=0)
     got_p[me] = jnp.concatenate([partial[:, :half], partial[:, half:]], axis=0).astype(bf16)
     pl.semaphore_wait(pltpu.get_barrier_semaphore(), len(rings) + len(cross))
-    out = []
-    for r, place in enumerate(rings):
-        out.append(send(got_p.at[me], got_p.at[me], sent_p.at[r], recv_p.at[me], on_mesh(sp=place)))
-        out[-1].start()
+    for place in rings:
+        send(got_p.at[me], got_p.at[me], sent_p, recv_p, on_mesh(sp=place)).start()
 
     gate_w[2 * gates_rows :, :] = jnp.zeros((gate_w.shape[0] - 2 * gates_rows, gate_w.shape[1]), bf16)
     for copy in row_loads:
@@ -252,36 +257,38 @@
 
     lax.fori_loop(0, total_tokens // 32, measure_rows, 0)
 
-    for place in rings:
-        spot = got_p.at[place]
-        send(spot, spot, sent_p.at[0], recv_p.at[place], on_mesh(sp=place)).wait_recv()
+    arrived(got_p.at[pl.ds(0, sp - 1)], recv_p)
     total = got_p[0].astype(f32)
     for place in range(1, sp):
         total = total + got_p[place].astype(f32)
     blocks[col] = jnp.concatenate([total[0:4], total[8:12]], axis=0)
     gate_row[...] = jnp.concatenate([total[4:5], total[12:13]], axis=1)
-    for r, place in enumerate(cross):
-        out.append(send(blocks.at[col], blocks.at[col], sent_t.at[r], recv_t.at[col], on_mesh(tp=place)))
-        out[-1].start()
     for place in cross:
-        spot = blocks.at[place]
-        send(spot, spot, sent_t.at[0], recv_t.at[place], on_mesh(tp=place)).wait_recv()
+        send(blocks.at[col], blocks.at[col], sent_t, recv_t, on_mesh(tp=place)).start()
+    arrived(blocks.at[pl.ds(0, tp - 1)], recv_t)
     for place in range(tp):
         at = place * width
         for part in range(2):
             lanes = slice(at + part * half, at + (part + 1) * half)
             four = blocks[place, 4 * part : 4 * part + 4, :]
-            st[0:2, lanes] = four[0:2]
-            st[2:4, lanes] = (1.0 + four[2:4]) * gain_ref[:, lanes]
+            scaled = (1.0 + four[2:4]) * gain_ref[:, lanes]
+            for which in range(2):
+                st[which, :, lanes] = jnp.broadcast_to(four[which : which + 1], (8, half))
+                st[2 + which, :, lanes] = jnp.broadcast_to(scaled[which : which + 1], (8, half))
 
     def modulate(first, count, which):
         def step(i, unused):
-            at = pl.ds(pl.multiple_of(first + i * 16, 16), 16)
-            values = rows_v[at, :].astype(f32) * stats[at, 0:1]
-            mod_v[at, :] = (values * st[2 + which : 3 + which, :] + st[which : which + 1, :]).astype(bf16)
+            at = pl.ds(pl.multiple_of(first + i * 32, 32), 32)
+            root = stats[at, :]
+            for lane_at in range(0, rows_v.shape[1], HEAD_DIM):
+                lanes = slice(lane_at, lane_at + HEAD_DIM)
+                values = rows_v[at, lanes].astype(f32) * root
+                shift, scale = st[which, :, lanes], st[2 + which, :, lanes]
+                parts = [values[n : n + 8] * scale + shift for n in range(0, 32, 8)]
+                mod_v[at, lanes] = jnp.concatenate(parts, axis=0).astype(bf16)
             return unused
 
-        lax.fori_loop(0, count // 16, step, 0)
+        lax.fori_loop(0, count // 32, step, 0)
 
     modulate(tokens, ctx_tokens, 1)
     modulate(0, tokens, 0)
@@ -356,12 +363,12 @@
         item, piece = owner // split, lax.rem(owner, split)
         return (
             send(
-                maps_m.at[part, item], got_m.at[part, me], sent_m.at[part, owner], recv_m.at[part, me],
+                maps_m.at[part, item], got_m.at[part, me], sent_m.at[part], recv_m.at[part],
                 on_mesh(sp=owner),
             ),
             send(
                 maps_b.at[part, item, pl.ds(pl.multiple_of(piece * part_rows, part_rows), part_rows)],
-                got_b.at[part, me], sent_b.at[part, owner], recv_b.at[part, me], on_mesh(sp=owner),
+                got_b.at[part, me], sent_b.at[part], recv_b.at[part], on_mesh(sp=owner),
             ),
         )
 
@@ -407,11 +414,8 @@
     reverse = lax.rem(my_item, 2)
 
     def arrive(part):
-        for place in rings:
-            spot = got_m.at[part, place]
-            send(spot, spot, sent_m.at[part, 0], recv_m.at[part, place], on_mesh(sp=place)).wait_recv()
-            spot = got_b.at[part, place]
-            send(spot, spot, sent_b.at[part, 0], recv_b.at[part, place], on_mesh(sp=place)).wait_recv()
+        arrived(got_m.at[part, pl.ds(0, sp - 1)], recv_m.at[part])
+        arrived(got_b.at[part, pl.ds(0, sp - 1)], recv_b.at[part])
 
     arrive(0)
     state = jnp.zeros((part_rows, HEAD_DIM), f32)
@@ -427,7 +431,7 @@
     back[me] = starts[me]
 
     def give_back(place):
-        return send(starts.at[place], back.at[me], sent_s.at[place], recv_s.at[me], on_mesh(sp=place))
+        return send(starts.at[place], back.at[me], sent_s, recv_s.at[my_item // 2], on_mesh(sp=place))
 
     for place in rings:
         give_back(place).start()
@@ -446,65 +450,66 @@
 
     def to_up(head, part):
         return send(
-            piece(head, col, part), piece(head, col, part), sent_up.at[head, part], recv_dn.at[head, part],
+            piece(head, col, part), piece(head, col, part), sent_o.at[head], recv_dn.at[head, part],
             on_mesh(tp=up),
         )
 
     def to_down(head, part):
         return send(
-            piece(head, col, part), piece(head, col, part), sent_dn.at[head, part], recv_up.at[head, part],
+            piece(head, col, part), piece(head, col, part), sent_o.at[head], recv_up.at[head, part],
             on_mesh(tp=down),
         )
 
     def forward(head, part):
         src, dst = (down, up) if part == 0 else (up, down)
         return send(
-            piece(head, src, part), piece(head, src, part), sent_f.at[head, part], recv_f.at[head, part],
+            piece(head, src, part), piece(head, src, part), sent_o.at[head], recv_f.at[head, part],
             on_mesh(tp=dst),
         )
 
     def relay(head, n, spot):
-        return send(spot, spot, sent_c.at[head, n], recv_c.at[head, n], on_mesh(tp=partner))
+        return send(spot, spot, sent_o.at[head], recv_c.at[head, n], on_mesh(tp=partner))
 
     def finish_head(head):
         half_items = [2 * head, 2 * head + 1]
-        for owner in range(2 * head * split, 2 * (head + 1) * split):
-
-            @pl.when(owner != me)
-            def _():
-                spot = back.at[owner]
-                send(spot, spot, sent_s.at[owner], recv_s.at[owner], on_mesh(sp=owner)).wait_recv()
+        @pl.when(me // half_owners == head)
+        def _():
+            arrived(back.at[pl.ds(0, half_owners - 1)], recv_s.at[head])
+
+        @pl.when(me // half_owners != head)
+        def _():
+            arrived(back.at[pl.ds(0, half_owners)], recv_s.at[head])
 
         pair = [back[item * split : (item + 1) * split].reshape(HEAD_DIM, HEAD_DIM) for item in half_items]
         combined = o_v[head] + mm_t(e_v[head], jnp.concatenate(pair, axis=1))
         norm = lax.rsqrt(jnp.mean(combined * combined, axis=1, keepdims=True) + epsilon)
         got_o[head, col] = (combined * norm * head_gain_ref[...]).astype(bf16)
         for copy in (to_up(head, 0), to_down(head, 1), to_up(head, 1), to_down(head, 0)):
-            out.append(copy)
             copy.start()
-        out.append(relay(head, 0, got_o.at[head, col]))
-        out[-1].start()
+        relay(head, 0, got_o.at[head, col]).start()
 
     def near_arrivals(head):
-        waits = ((down, 0, recv_dn, True), (up, 1, recv_up, True), (down, 1, recv_dn, False), (up, 0, recv_up, False))
-        for n, (place, part, sems, onward) in enumerate(waits):
+        waits = (
+            (down, 0, recv_dn, 1, True),
+            (up, 1, recv_up, 2, True),
+            (down, 1, recv_dn, 1, False),
+            (up, 0, recv_up, 2, False),
+        )
+        for place, part, sems, n, onward in waits:
             spot = piece(head, place, part)
-            send(spot, spot, sent_up.at[head, part], sems.at[head, part], on_mesh(tp=place)).wait_recv()
+            arrived(spot, sems.at[head, part])
             if onward:
-                out.append(forward(head, part))
-                out[-1].start()
-            out.append(relay(head, 1 + n, spot))
-            out[-1].start()
+                forward(head, part).start()
+            relay(head, n, spot).start()
 
     def far_arrivals(head):
         for part in range(2):
             spot = piece(head, far, part)
-            send(spot, spot, sent_f.at[head, part], recv_f.at[head, part], on_mesh(tp=up)).wait_recv()
-            out.append(relay(head, 5 + part, spot))
-            out[-1].start()
-
-    def from_partner(head, n, spot):
-        send(spot, spot, sent_c.at[head, n], recv_c.at[head, n], on_mesh(tp=partner)).wait_recv()
+            arrived(spot, recv_f.at[head, part])
+            relay(head, 3, spot).start()
+
+    def from_partner(head, n):
+        arrived(got_o.at[head, 0], recv_c.at[head, n])
 
     def add(head, place, first=False):
         even = place - core
@@ -521,18 +526,15 @@
         acc[...] = part if first else acc[...] + part
 
     def near_matmuls(head):
-        from_partner(head, 0, got_o.at[head, partner])
+        from_partner(head, 0)
         add(head, col, head == 0)
-        other = 1 - 2 * core
-        for n, (place, part) in enumerate(((down, 0), (up, 1), (down, 1), (up, 0))):
-            from_partner(head, 1 + n, piece(head, place + other, part))
+        from_partner(head, 1)
         add(head, down)
+        from_partner(head, 2)
         add(head, up)
 
     def far_matmuls(head):
-        other = 1 - 2 * core
-        for part in range(2):
-            from_partner(head, 5 + part, piece(head, far + other, part))
+        from_partner(head, 3)
         add(head, far)
 
     out_load.wait()
@@ -549,14 +551,14 @@
     far_matmuls(heads - 1)
     lanes = pl.ds(pl.multiple_of(col * width, width), width)
     out_ref[...] = rows_v[0:tokens, lanes].astype(f32) + gate_row[...] * acc[...]
-    for copy in out:
-        copy.wait_send()
+    left(got_p.at[pl.ds(0, sp - 1)], sent_p)
+    left(blocks.at[pl.ds(0, tp - 1)], sent_t)
     for part in range(2):
-        for r in range(1, sp):
-            for copy in ship(part, lax.rem(me + r, sp)):
-                copy.wait_send()
-    for place in rings:
-        give_back(place).wait_send()
+        left(got_m.at[part, pl.ds(0, sp - 1)], sent_m.at[part])
+        left(got_b.at[part, pl.ds(0, sp - 1)], sent_b.at[part])
+    left(starts.at[pl.ds(0, sp - 1)], sent_s)
+    for head in range(heads):
+        left(got_o.at[head, pl.ds(0, tp - 1)], sent_o.at[head])
 
 
 def body(
@@ -592,7 +594,7 @@
     chunks = sum(len(part) for part in spans(tokens, ctx_tokens))
     vmem = pl.BlockSpec(memory_space=pltpu.VMEM)
     smem = pl.BlockSpec(memory_space=pltpu.SMEM)
-    anywhere = pl.BlockSpec(memory_space=pl.ANY)
+    anywhere = pl.BlockSpec(memory_space=pltpu.HBM)
     dma = pltpu.SemaphoreType.DMA
     flat = [jnp.transpose(w, (1, 2, 0)).reshape(-1, features) for w in (write_weight, decay_weight)]
     updated = pl.pallas_call(
@@ -608,7 +610,7 @@
             pltpu.VMEM(value_weight.shape, bf16),
             pltpu.VMEM((HEAD_DIM, features), bf16),
             pltpu.VMEM(out_weight.shape, bf16),
-            pltpu.VMEM((4, features), f32),
+            pltpu.VMEM((4, 8, features), f32),
             pltpu.VMEM((total, HEAD_DIM), f32),
             pltpu.VMEM((total, features), bf16),
             pltpu.VMEM((tokens, inner), bf16),
@@ -631,27 +633,24 @@
             pltpu.VMEM((heads, tp, tokens, HEAD_DIM), bf16),
             pltpu.VMEM((tokens, width), f32),
             dma((11,)),
-            dma((sp,)),
-            dma((sp,)),
-            dma((tp,)),
-            dma((tp,)),
-            dma((2, sp)),
-            dma((2, sp)),
-            dma((2, sp)),
-            dma((2, sp)),
-            dma((sp,)),
-            dma((sp,)),
+            dma,
+            dma,
+            dma,
+            dma,
+            dma((2,)),
+            dma((2,)),
+            dma((2,)),
+            dma((2,)),
+            dma,
+            dma((heads,)),
+            dma((heads,)),
             dma((heads, 2)),
             dma((heads, 2)),
             dma((heads, 2)),
-            dma((heads, 2)),
-            dma((heads, 2)),
-            dma((heads, 2)),
-            dma((heads, 7)),
-            dma((heads, 7)),
+            dma((heads, 4)),
         ],
         compiler_params=pltpu.CompilerParams(
-            collective_id=0, has_side_effects=True, vmem_limit_bytes=56 * 1024 * 1024
+            collective_id=0, has_side_effects=True, vmem_limit_bytes=58 * 1024 * 1024
         ),
         name="mixer",
     )(

time: 75.1 us -> 70.2 us (0.935)
  Pallas kernels: 72.8 us -> 67.9 us
    pallas_call x1, Pallas kernels: 72.8 us -> 67.9 us  [body(): pl.pallas_call(functools.partial(mixer_kernel, sp, tp, heads, tokens, ctx...]
where the time goes in v2:
time: 70.2 us; the launch traced here: 70 us
  Pallas kernels  67.9 us (97%)
  other arithmetic  2.08 us (3%)
    pallas_call x1, Pallas kernels, body(): pl.pallas_call(functools.partial(mixer_kernel, sp, tp, heads, tokens, ctx...  67.9 us
    convert_element_type x1, other arithmetic, body(): return updated.astype(bf16)  2.08 us

profile of v2, /device:TPU:1, one launch (start us, length us, event | category | flops | bytes accessed | tf_op | source)
XLA Modules:
  0.0 70.0 jit_solution(1266293388531887684)
XLA Ops:
  0.0 67.9 %mixer.1 = f32[512,512]{1,0:T(8,128)} custom-call(bf16[2,128]{1,0:T(2,128)(2,1)} %bitcast.13, bf16[2,128]{1,0:T(2,128)(2,1)} %bitcast.14, f32[1,4096]{1,0:T(1,128)} %bitcast.12, f32[1,128]{1,0:T(1,128)} %bitcast.15, f32[2,16]{1,0:T(2,128)} %write_bias_ref.1, f32[2,16]{1,0:T(2,128)} %decay_bias_ref.1, f32[2,16]{1,0:T(2,128)} %log_rate_ref.1, ...), custom_call_target="tpu_custom_call" | custom-call | tf_op jit(solution)/shard_map/mixer/pallas_call | solution.py:600
  67.9 2.1 %convert_element_type.3 = bf16[512,512]{1,0:T(8,128)(2,1)} convert(f32[512,512]{1,0:T(8,128)} %mixer.1) | non-fusion elementwise | flops 262144 | bytes 1572864 | tf_op jit(solution)/shard_map/convert_element_type | solution.py:676

commit v3 on v2

--- a/solution.py
+++ b/solution.py
@@ -51,13 +51,6 @@
         group["keys"] = keys.astype(f32) * s_col
         group["keys_t"] = keys_t * s_row
         group["values"] = group["v"].astype(f32)
-        if group["q"] is not None:
-            queries = group["q"].astype(f32)
-            q_scale = lax.rsqrt(jnp.sum(queries * queries, axis=1, keepdims=True) + epsilon) * HEAD_DIM**-0.5
-            group["queries"] = queries * q_scale
-            group["score"] = (
-                jnp.dot(group["q"], keys_t.astype(bf16), preferred_element_type=f32) * q_scale * s_row
-            )
         for d in range(2):
             rate_col, run_col, run_row = group["gates"][d]
             inside = rows >= cols if d == 0 else rows <= cols
@@ -66,8 +59,6 @@
             system = jnp.where(strict, gram * decay * rate_col, 0.0)
             item = dict(group=group, size=size, d=d, rate_col=rate_col, run_col=run_col, run_row=run_row)
             item["system"] = system
-            if group["q"] is not None:
-                item["score"] = group["score"] * decay
             near = (rows // 2) == (cols // 2)
             item["inv"] = jnp.where(rows == cols, 1.0, jnp.where(near, -system, 0.0))
             items.append(item)
@@ -100,35 +91,115 @@
         item["gate"] = jnp.exp(last)
         late_t = group["keys_t"] * jnp.exp(last - item["run_row"])
         item["late"] = mm(late_t, item["solved"])
-        if group["q"] is not None:
-            weighed = mm(item["score"], item["solved"])
-            item["local"] = weighed[:, :HEAD_DIM]
-            item["early"] = group["queries"] * growth - weighed[:, HEAD_DIM:]
     return items
 
 
-def chain(items, d, e_ref):
+def solve_groups(groups):
+    size = groups[0]["size"]
+    rows, cols = iotas(size)
+    near = (rows // 2) == (cols // 2)
+    for group in groups:
+        keys = group["k"]
+        keys_t = keys.astype(f32).T
+        group["plain_t"] = keys_t.astype(bf16)
+        gram = jnp.dot(keys, group["plain_t"], preferred_element_type=f32)
+        diag = jnp.where(rows == cols, gram, 0.0)
+        s_col = lax.rsqrt(jnp.sum(diag, axis=1, keepdims=True) + epsilon)
+        s_row = lax.rsqrt(jnp.sum(diag, axis=0, keepdims=True) + epsilon)
+        gram = gram * s_col * s_row
+        group["s_row"] = s_row
+        group["keys"] = keys.astype(f32) * s_col
+        group["keys_t"] = keys_t * s_row
+        group["decay"], group["system"], group["inv"] = [], [], []
+        for d in range(2):
+            rate_col, run_col, run_row = group["gates"][d]
+            inside = rows >= cols if d == 0 else rows <= cols
+            strict = rows > cols if d == 0 else rows < cols
+            decay = jnp.where(inside, jnp.exp(jnp.minimum(run_col - run_row, 0.0)), 0.0)
+            group["decay"].append(decay)
+            system = jnp.where(strict, gram * decay * rate_col, 0.0)
+            group["system"].append(system.astype(bf16))
+            group["inv"].append(jnp.where(rows == cols, 1.0, jnp.where(near, -system, 0.0)))
+    span = 2
+    while span < size:
+        row_block, col_block = rows // span, cols // span
+        masks = (
+            ((row_block % 2) == 1) & (col_block == row_block - 1),
+            ((col_block % 2) == 1) & (row_block == col_block - 1),
+        )
+        masks = [jnp.where(mask, 1.0, 0.0).astype(bf16) for mask in masks]
+        firsts = []
+        for group in groups:
+            group["packed"] = [inv.astype(bf16) for inv in group["inv"]]
+            firsts.append([mm(group["system"][d] * masks[d], group["packed"][d]) for d in range(2)])
+        for group, first in zip(groups, firsts):
+            group["inv"] = [group["inv"][d] - mm(group["packed"][d], first[d]) for d in range(2)]
+        span *= 2
+    for group in groups:
+        values = group["v"].astype(f32)
+        group["growth"], group["solved"], group["late"], group["gate"] = [], [], [], []
+        for d in range(2):
+            rate_col, run_col, run_row = group["gates"][d]
+            growth = jnp.exp(run_col)
+            both = jnp.concatenate([values * rate_col, group["keys"] * (rate_col * growth)], axis=1)
+            solved = mm(group["inv"][d], both).astype(bf16)
+            last = run_row[:, size - 1 :] if d == 0 else run_row[:, :1]
+            group["growth"].append(growth)
+            group["solved"].append(solved)
+            group["gate"].append(jnp.exp(last))
+            group["late"].append(mm(group["keys_t"] * jnp.exp(last - run_row), solved))
+
+
+def follow(carry, late, gate, eye):
+    fresh = jnp.concatenate([late[:, :HEAD_DIM], (gate - 1.0) * eye - late[:, HEAD_DIM:]], axis=1)
+    if carry is None:
+        return fresh
+    return gate * carry + fresh - mm(late[:, HEAD_DIM:], carry)
+
+
+def identity():
     rows, cols = iotas(HEAD_DIM)
-    eye = (rows == cols).astype(f32)
+    return (rows == cols).astype(f32)
+
+
+def chain(items, d):
+    eye = identity()
     carry = None
     for item in items if d == 0 else items[::-1]:
-        if e_ref is not None:
-            if carry is None:
-                out, early = item["local"], item["early"]
-            else:
-                moved = mm(item["early"], carry)
-                out = item["local"] + moved[:, :HEAD_DIM]
-                early = item["early"] + moved[:, HEAD_DIM:]
-            at, size = item["group"]["at"], item["size"]
+        carry = follow(carry, item["late"], item["gate"], eye)
+    return carry
+
+
+def chain_groups(groups, d):
+    eye = identity()
+    carry = None
+    for group in groups if d == 0 else groups[::-1]:
+        group["before", d] = None if carry is None else carry.astype(bf16)
+        carry = follow(carry, group["late"][d], group["gate"][d], eye)
+    return carry
+
+
+def outputs(groups, q_of, o_ref, e_ref):
+    for group in groups:
+        at, size = group["at"], group["size"]
+        plain = q_of(at, size)
+        queries = plain.astype(f32)
+        q_scale = lax.rsqrt(jnp.sum(queries * queries, axis=1, keepdims=True) + epsilon) * HEAD_DIM**-0.5
+        queries = queries * q_scale
+        score = jnp.dot(plain, group["plain_t"], preferred_element_type=f32) * q_scale * group["s_row"]
+        total = None
+        for d in range(2):
+            weighed = mm(score * group["decay"][d], group["solved"][d])
+            out = weighed[:, :HEAD_DIM]
+            early = queries * group["growth"][d] - weighed[:, HEAD_DIM:]
+            before = group["before", d]
+            if before is not None:
+                moved = mm(early, before)
+                out = out + moved[:, :HEAD_DIM]
+                early = early + moved[:, HEAD_DIM:]
             e_ref[at : at + size, d * HEAD_DIM : (d + 1) * HEAD_DIM] = early.astype(bf16)
-            item["out"] = out
-        late, gate = item["late"], item["gate"]
-        fresh = jnp.concatenate([late[:, :HEAD_DIM], (gate - 1.0) * eye - late[:, HEAD_DIM:]], axis=1)
-        if carry is None:
-            carry = fresh
-        else:
-            carry = gate * carry + fresh - mm(late[:, HEAD_DIM:], carry)
-    return carry
+            total = out if total is None else total + out
+        o_ref[at : at + size, :] = total
 
 
 def on_mesh(sp=None, tp=None):
@@ -182,9 +253,10 @@
 ):
     me, col = lax.axis_index("sp"), lax.axis_index("tp")
     items = 2 * heads
-    split = sp // items
+    quads = sp // items
+    split = 2
     part_rows = HEAD_DIM // split
-    half_owners = sp // heads
+    core = lax.rem(col, 2)
     width = mod_w.shape[2]
     half = width // 2
     total_tokens = tokens + ctx_tokens
@@ -297,7 +369,6 @@
     pre = mm_t(mod_v[...], gate_w[...]).astype(bf16).astype(f32)
     k_v[...] = jnp.dot(mod_v[...], k_w[...], preferred_element_type=f32).astype(bf16)
     v_v[...] = jnp.dot(mod_v[...], v_w[...], preferred_element_type=f32).astype(bf16)
-    q_v[...] = jnp.dot(mod_v[0:tokens, :], q_w[...], preferred_element_type=f32).astype(bf16)
 
     all_heads = gates_rows // 2
     first_head = col * heads
@@ -331,7 +402,7 @@
         run_v[at : at + size, :] = running
         run_t[n, :, :size] = running.T
 
-    def group_of(n, at, size, head, latent):
+    def group_of(n, at, size, head):
         lanes = slice(head * HEAD_DIM, (head + 1) * HEAD_DIM)
         gates = []
         for d in range(2):
@@ -349,7 +420,6 @@
             size=size,
             k=k_v[at : at + size, lanes],
             v=v_v[at : at + size, lanes],
-            q=q_v[at : at + size, lanes] if latent else None,
             gates=gates,
         )
 
@@ -357,86 +427,90 @@
         maps_b[part, item] = carry[:, :HEAD_DIM].T.astype(bf16)
         maps_m[part, item] = carry[:, HEAD_DIM:].T.astype(bf16)
 
-    my_item, my_part = me // split, lax.rem(me, split)
-
-    def ship(part, owner):
-        item, piece = owner // split, lax.rem(owner, split)
-        return (
+    def owner_of(item, piece):
+        return item * quads + 2 * piece + lax.rem(item + core, 2)
+
+    my_item, my_part = me // quads, lax.rem(me, quads) // 2
+    owning = lax.rem(me, 2) == lax.rem(my_item + core, 2)
+    reverse = lax.rem(my_item, 2)
+
+    def ship(part, item, piece):
+        owner = owner_of(item, piece)
+
+        @pl.when(owner != me)
+        def _():
             send(
-                maps_m.at[part, item], got_m.at[part, me], sent_m.at[part], recv_m.at[part],
-                on_mesh(sp=owner),
-            ),
+                maps_m.at[part, item], got_m.at[part, me], sent_m.at[part], recv_m.at[part], on_mesh(sp=owner)
+            ).start()
             send(
-                maps_b.at[part, item, pl.ds(pl.multiple_of(piece * part_rows, part_rows), part_rows)],
+                maps_b.at[part, item, pl.ds(piece * part_rows, part_rows)],
                 got_b.at[part, me], sent_b.at[part], recv_b.at[part], on_mesh(sp=owner),
-            ),
-        )
+            ).start()
 
     def ship_head(part, head):
-        base = head * half_owners
-        for r in range(1, half_owners):
-            for copy in ship(part, base + lax.rem(me + r, half_owners)):
-                copy.start()
-
-        @pl.when(me // half_owners != head)
-        def _():
-            for copy in ship(part, base + lax.rem(me, half_owners)):
-                copy.start()
+        for item in (2 * head, 2 * head + 1):
+            for piece in range(split):
+                ship(part, item, piece)
 
     def keep_own(part):
         got_m[part, me] = maps_m[part, my_item]
         got_b[part, me] = maps_b[part, my_item, pl.ds(pl.multiple_of(my_part * part_rows, part_rows), part_rows), :]
 
-    ctx_items = {}
     ctx_groups = []
     for head in range(heads):
         for n, (at, size) in enumerate(ctx):
-            ctx_groups.append(group_of(len(lat) + n, at, size, head, False))
+            ctx_groups.append(group_of(len(lat) + n, at, size, head))
     done = prepare(ctx_groups)
     each = 2 * len(ctx)
     for head in range(heads):
         for d in range(2):
             chosen = [i for i in done[head * each : (head + 1) * each] if i["d"] == d]
-            keep(0, 2 * head + d, chain(chosen, d, None))
+            keep(0, 2 * head + d, chain(chosen, d))
     for head in range(heads):
         ship_head(0, head)
+    latents = []
     for head in range(heads):
-        done = prepare([group_of(n, at, size, head, True) for n, (at, size) in enumerate(lat)])
+        latents.append([group_of(n, at, size, head) for n, (at, size) in enumerate(lat)])
+        solve_groups(latents[head])
         for d in range(2):
-            keep(1, 2 * head + d, chain([i for i in done if i["d"] == d], d, e_v.at[head]))
-        for at, size in lat:
-            pair = [i for i in done if i["group"]["at"] == at]
-            o_v[head, at : at + size, :] = pair[0]["out"] + pair[1]["out"]
+            keep(1, 2 * head + d, chain_groups(latents[head], d))
         ship_head(1, head)
-    keep_own(0)
-    keep_own(1)
-
-    reverse = lax.rem(my_item, 2)
+    q_v[...] = jnp.dot(mod_v[0:tokens, :], q_w[...], preferred_element_type=f32).astype(bf16)
+    for head in range(heads):
+
+        def q_of(at, size):
+            return q_v[at : at + size, head * HEAD_DIM : (head + 1) * HEAD_DIM]
+
+        outputs(latents[head], q_of, o_v.at[head], e_v.at[head])
 
     def arrive(part):
         arrived(got_m.at[part, pl.ds(0, sp - 1)], recv_m.at[part])
         arrived(got_b.at[part, pl.ds(0, sp - 1)], recv_b.at[part])
 
-    arrive(0)
-    state = jnp.zeros((part_rows, HEAD_DIM), f32)
-    for step in range(sp):
-        place = step + reverse * (sp - 1 - 2 * step)
-        state = advance(state, got_m[0, place], got_b[0, place])
-    arrive(1)
-    for step in range(sp):
-        place = step + reverse * (sp - 1 - 2 * step)
-        starts[place] = state.astype(bf16)
-        if step < sp - 1:
-            state = advance(state, got_m[1, place], got_b[1, place])
-    back[me] = starts[me]
-
     def give_back(place):
-        return send(starts.at[place], back.at[me], sent_s, recv_s.at[my_item // 2], on_mesh(sp=place))
-
-    for place in rings:
-        give_back(place).start()
-
-    core = lax.rem(col, 2)
+        return send(
+            starts.at[place], back.at[my_item * split + my_part], sent_s, recv_s.at[my_item // 2], on_mesh(sp=place)
+        )
+
+    @pl.when(owning)
+    def _():
+        keep_own(0)
+        keep_own(1)
+        arrive(0)
+        state = jnp.zeros((part_rows, HEAD_DIM), f32)
+        for step in range(sp):
+            place = step + reverse * (sp - 1 - 2 * step)
+            state = advance(state, got_m[0, place], got_b[0, place])
+        arrive(1)
+        for step in range(sp):
+            place = step + reverse * (sp - 1 - 2 * step)
+            starts[place] = state.astype(bf16)
+            if step < sp - 1:
+                state = advance(state, got_m[1, place], got_b[1, place])
+        for place in rings:
+            give_back(place).start()
+        back[my_item * split + my_part] = starts[me]
+
     chips = tp // 2
     chip = col // 2
     partner = col + 1 - 2 * core
@@ -472,13 +546,15 @@
 
     def finish_head(head):
         half_items = [2 * head, 2 * head + 1]
-        @pl.when(me // half_owners == head)
+        mine = owning & (my_item // 2 == head)
+
+        @pl.when(mine)
         def _():
-            arrived(back.at[pl.ds(0, half_owners - 1)], recv_s.at[head])
-
-        @pl.when(me // half_owners != head)
+            arrived(back.at[pl.ds(0, 2 * split - 1)], recv_s.at[head])
+
+        @pl.when(jnp.logical_not(mine))
         def _():
-            arrived(back.at[pl.ds(0, half_owners)], recv_s.at[head])
+            arrived(back.at[pl.ds(0, 2 * split)], recv_s.at[head])
 
         pair = [back[item * split : (item + 1) * split].reshape(HEAD_DIM, HEAD_DIM) for item in half_items]
         combined = o_v[head] + mm_t(e_v[head], jnp.concatenate(pair, axis=1))
@@ -553,10 +629,21 @@
     out_ref[...] = rows_v[0:tokens, lanes].astype(f32) + gate_row[...] * acc[...]
     left(got_p.at[pl.ds(0, sp - 1)], sent_p)
     left(blocks.at[pl.ds(0, tp - 1)], sent_t)
-    for part in range(2):
-        left(got_m.at[part, pl.ds(0, sp - 1)], sent_m.at[part])
-        left(got_b.at[part, pl.ds(0, sp - 1)], sent_b.at[part])
-    left(starts.at[pl.ds(0, sp - 1)], sent_s)
+
+    def sent_maps(count):
+        for part in range(2):
+            left(got_m.at[part, pl.ds(0, count)], sent_m.at[part])
+            left(got_b.at[part, pl.ds(0, count)], sent_b.at[part])
+
+    @pl.when(owning)
+    def _():
+        sent_maps(items * split - 1)
+        left(starts.at[pl.ds(0, sp - 1)], sent_s)
+
+    @pl.when(jnp.logical_not(owning))
+    def _():
+        sent_maps(items * split)
+
     for head in range(heads):
         left(got_o.at[head, pl.ds(0, tp - 1)], sent_o.at[head])
 
@@ -589,7 +676,7 @@
     features = latent.shape[1]
     width = shift_weight.shape[1]
     items = 2 * heads
-    split = sp // items
+    split = 2
     rows = HEAD_DIM // split
     chunks = sum(len(part) for part in spans(tokens, ctx_tokens))
     vmem = pl.BlockSpec(memory_space=pltpu.VMEM)
@@ -629,7 +716,7 @@
             pltpu.VMEM((2, sp, HEAD_DIM, HEAD_DIM), bf16),
             pltpu.VMEM((2, sp, rows, HEAD_DIM), bf16),
             pltpu.VMEM((sp, rows, HEAD_DIM), bf16),
-            pltpu.VMEM((sp, rows, HEAD_DIM), bf16),
+            pltpu.VMEM((items * split, rows, HEAD_DIM), bf16),
             pltpu.VMEM((heads, tp, tokens, HEAD_DIM), bf16),
             pltpu.VMEM((tokens, width), f32),
             dma((11,)),

time: 70.2 us -> 65.5 us (0.933)
  Pallas kernels: 67.9 us -> 63.2 us
    pallas_call x1, Pallas kernels: 67.9 us -> 63.2 us  [body(): pl.pallas_call(functools.partial(mixer_kernel, sp, tp, heads, tokens, ctx...]
where the time goes in v3:
time: 65.5 us; the launch traced here: 65.3 us
  Pallas kernels  63.2 us (96%)
  other arithmetic  2.08 us (3%)
    pallas_call x1, Pallas kernels, body(): pl.pallas_call(functools.partial(mixer_kernel, sp, tp, heads, tokens, ctx...  63.2 us
    convert_element_type x1, other arithmetic, body(): return updated.astype(bf16)  2.08 us

profile of v3, /device:TPU:1, one launch (start us, length us, event | category | flops | bytes accessed | tf_op | source)
XLA Modules:
  0.0 65.3 jit_solution(11113327020041463568)
XLA Ops:
  0.0 63.2 %mixer.1 = f32[512,512]{1,0:T(8,128)} custom-call(bf16[2,128]{1,0:T(2,128)(2,1)} %bitcast.13, bf16[2,128]{1,0:T(2,128)(2,1)} %bitcast.14, f32[1,4096]{1,0:T(1,128)} %bitcast.12, f32[1,128]{1,0:T(1,128)} %bitcast.15, f32[2,16]{1,0:T(2,128)} %write_bias_ref.1, f32[2,16]{1,0:T(2,128)} %decay_bias_ref.1, f32[2,16]{1,0:T(2,128)} %log_rate_ref.1, ...), custom_call_target="tpu_custom_call" | custom-call | tf_op jit(solution)/shard_map/mixer/pallas_call | solution.py:687
  63.2 2.1 %convert_element_type.3 = bf16[512,512]{1,0:T(8,128)(2,1)} convert(f32[512,512]{1,0:T(8,128)} %mixer.1) | non-fusion elementwise | flops 262144 | bytes 1572864 | tf_op jit(solution)/shard_map/convert_element_type | solution.py:763

commit v4 on v3

--- a/solution.py
+++ b/solution.py
@@ -247,7 +247,7 @@
     write_hbm, decay_hbm, out_hbm,
     out_ref,
     rows_v, mod_w, q_w, k_w, v_w, gate_w, out_w, st, stats, mod_v, q_v, k_v, v_v, rate_v, run_v, run_t,
-    got_p, blocks, gate_row, o_v, e_v, maps_m, maps_b, got_m, got_b, starts, back, got_o, acc,
+    got_p, blocks, gate_row, ctx_state, o_v, e_v, maps_m, maps_b, got_m, got_b, starts, back, got_o, acc,
     load, sent_p, recv_p, sent_t, recv_t, sent_m, recv_m, sent_b, recv_b, sent_s, recv_s,
     sent_o, recv_dn, recv_up, recv_f, recv_c,
 ):
@@ -257,6 +257,12 @@
     split = 2
     part_rows = HEAD_DIM // split
     core = lax.rem(col, 2)
+    chips = tp // 2
+    chip = col // 2
+    partner = col + 1 - 2 * core
+    up = lax.rem(chip + 1, chips) * 2 + core
+    down = lax.rem(chip + chips - 1, chips) * 2 + core
+    far = lax.rem(chip + 2, chips) * 2 + core
     width = mod_w.shape[2]
     half = width // 2
     total_tokens = tokens + ctx_tokens
@@ -475,14 +481,6 @@
         for d in range(2):
             keep(1, 2 * head + d, chain_groups(latents[head], d))
         ship_head(1, head)
-    q_v[...] = jnp.dot(mod_v[0:tokens, :], q_w[...], preferred_element_type=f32).astype(bf16)
-    for head in range(heads):
-
-        def q_of(at, size):
-            return q_v[at : at + size, head * HEAD_DIM : (head + 1) * HEAD_DIM]
-
-        outputs(latents[head], q_of, o_v.at[head], e_v.at[head])
-
     def arrive(part):
         arrived(got_m.at[part, pl.ds(0, sp - 1)], recv_m.at[part])
         arrived(got_b.at[part, pl.ds(0, sp - 1)], recv_b.at[part])
@@ -491,6 +489,25 @@
         return send(
             starts.at[place], back.at[my_item * split + my_part], sent_s, recv_s.at[my_item // 2], on_mesh(sp=place)
         )
+
+    def q_of(head):
+        lanes = slice(head * HEAD_DIM, (head + 1) * HEAD_DIM)
+        return lambda at, size: q_v[at : at + size, lanes]
+
+    def run_chain():
+        arrive(1)
+        state = ctx_state[...]
+        for step in range(sp):
+            place = step + reverse * (sp - 1 - 2 * step)
+            starts[place] = state.astype(bf16)
+            if step < sp - 1:
+                state = advance(state, got_m[1, place], got_b[1, place])
+        for place in rings:
+            give_back(place).start()
+        back[my_item * split + my_part] = starts[me]
+
+    q_v[...] = jnp.dot(mod_v[0:tokens, :], q_w[...], preferred_element_type=f32).astype(bf16)
+    outputs(latents[0], q_of(0), o_v.at[0], e_v.at[0])
 
     @pl.when(owning)
     def _():
@@ -501,22 +518,16 @@
         for step in range(sp):
             place = step + reverse * (sp - 1 - 2 * step)
             state = advance(state, got_m[0, place], got_b[0, place])
-        arrive(1)
-        for step in range(sp):
-            place = step + reverse * (sp - 1 - 2 * step)
-            starts[place] = state.astype(bf16)
-            if step < sp - 1:
-                state = advance(state, got_m[1, place], got_b[1, place])
-        for place in rings:
-            give_back(place).start()
-        back[my_item * split + my_part] = starts[me]
-
-    chips = tp // 2
-    chip = col // 2
-    partner = col + 1 - 2 * core
-    up = lax.rem(chip + 1, chips) * 2 + core
-    down = lax.rem(chip + chips - 1, chips) * 2 + core
-    far = lax.rem(chip + 2, chips) * 2 + core
+        ctx_state[...] = state
+
+    for head in range(heads):
+        if head > 0:
+            outputs(latents[head], q_of(head), o_v.at[head], e_v.at[head])
+
+        @pl.when(owning & (my_item // 2 == head))
+        def _():
+            run_chain()
+
     mid = tokens // 2
 
     def piece(head, place, part):
@@ -601,32 +612,25 @@
         part = jnp.dot(lanes, weights, preferred_element_type=f32)
         acc[...] = part if first else acc[...] + part
 
-    def near_matmuls(head):
+    out_load.wait()
+    for head in range(heads):
+        finish_head(head)
+    near_arrivals(0)
+    for head in range(heads):
         from_partner(head, 0)
         add(head, col, head == 0)
-        from_partner(head, 1)
-        add(head, down)
-        from_partner(head, 2)
-        add(head, up)
-
-    def far_matmuls(head):
+    for head in range(1, heads):
+        near_arrivals(head)
+    for head in range(heads):
+        for n, place in ((1, down), (2, up)):
+            from_partner(head, n)
+            add(head, place)
+        far_arrivals(head)
+    for head in range(heads):
         from_partner(head, 3)
         add(head, far)
-
-    out_load.wait()
-    finish_head(0)
-    near_arrivals(0)
-    for head in range(1, heads):
-        finish_head(head)
-        far_arrivals(head - 1)
-        near_matmuls(head - 1)
-        far_matmuls(head - 1)
-        near_arrivals(head)
-    far_arrivals(heads - 1)
-    near_matmuls(heads - 1)
-    far_matmuls(heads - 1)
     lanes = pl.ds(pl.multiple_of(col * width, width), width)
-    out_ref[...] = rows_v[0:tokens, lanes].astype(f32) + gate_row[...] * acc[...]
+    out_ref[...] = (rows_v[0:tokens, lanes].astype(f32) + gate_row[...] * acc[...]).astype(bf16)
     left(got_p.at[pl.ds(0, sp - 1)], sent_p)
     left(blocks.at[pl.ds(0, tp - 1)], sent_t)
 
@@ -646,6 +650,20 @@
 
     for head in range(heads):
         left(got_o.at[head, pl.ds(0, tp - 1)], sent_o.at[head])
+
+
+def deliver_kernel(src, dst, held, taken, given):
+    rows = held.shape[0] // 4
+    spots = [pl.ds(n * rows, rows) for n in range(4)]
+    takes = [pltpu.make_async_copy(src.at[spot], held.at[spot], taken.at[n]) for n, spot in enumerate(spots)]
+    gives = [pltpu.make_async_copy(held.at[spot], dst.at[spot], given.at[n]) for n, spot in enumerate(spots)]
+    for take in takes:
+        take.start()
+    for take, give in zip(takes, gives):
+        take.wait()
+        give.start()
+    for give in gives:
+        give.wait()
 
 
 def body(
@@ -688,7 +706,7 @@
         functools.partial(mixer_kernel, sp, tp, heads, tokens, ctx_tokens),
         in_specs=[vmem] * 4 + [smem] * 3 + [anywhere] * 11,
         out_specs=vmem,
-        out_shape=jax.ShapeDtypeStruct((tokens, width), f32),
+        out_shape=jax.ShapeDtypeStruct((tokens, width), bf16),
         scratch_shapes=[
             pltpu.VMEM((total, features), bf16),
             pltpu.VMEM((3,) + shift_weight.shape, bf16),
@@ -709,6 +727,7 @@
             pltpu.VMEM((sp, 16, width // 2), bf16),
             pltpu.VMEM((tp, 8, width // 2), f32),
             pltpu.VMEM((1, width), f32),
+            pltpu.VMEM((rows, HEAD_DIM), f32),
             pltpu.VMEM((heads, tokens, HEAD_DIM), f32),
             pltpu.VMEM((heads, tokens, 2 * HEAD_DIM), bf16),
             pltpu.VMEM((2, items, HEAD_DIM, HEAD_DIM), bf16),
@@ -760,7 +779,15 @@
         flat[1],
         out_weight,
     )
-    return updated.astype(bf16)
+    return pl.pallas_call(
+        deliver_kernel,
+        in_specs=[pl.BlockSpec(memory_space=pltpu.HBM)],
+        out_specs=pl.BlockSpec(memory_space=pltpu.HBM),
+        out_shape=jax.ShapeDtypeStruct((tokens, width), bf16),
+        scratch_shapes=[pltpu.VMEM((tokens, width), bf16), dma((4,)), dma((4,))],
+        compiler_params=pltpu.CompilerParams(vmem_limit_bytes=58 * 1024 * 1024),
+        name="deliver",
+    )(updated)
 
 
 def solution(mesh):

time: 65.5 us -> 61.9 us (0.945)
  other arithmetic: 2.08 us -> 0 us
  Pallas kernels: 63.2 us -> 61.6 us
    pallas_call x1, Pallas kernels: 63.2 us -> 59.8 us  [body(): pl.pallas_call(functools.partial(mixer_kernel, sp, tp, heads, tokens, ctx...]
    convert_element_type x1 -> x0, other arithmetic: 2.08 us -> none  [body(): return updated.astype(bf16)]
    pallas_call x0 -> x1, Pallas kernels: none -> 1.82 us  [body(): pl.pallas_call(deliver_kernel, in_specs=[pl.BlockSpec(memory_space=pltpu....]
where the time goes in v4:
time: 61.9 us; the launch traced here: 61.8 us
  Pallas kernels  61.6 us (100%)
    pallas_call x1, Pallas kernels, body(): pl.pallas_call(functools.partial(mixer_kernel, sp, tp, heads, tokens, ctx...  59.8 us
    pallas_call x1, Pallas kernels, body(): pl.pallas_call(deliver_kernel, in_specs=[pl.BlockSpec(memory_space=pltpu....  1.82 us

profile of v4, /device:TPU:1, one launch (start us, length us, event | category | flops | bytes accessed | tf_op | source)
XLA Modules:
  0.0 61.8 jit_solution(7971007999184566218)
XLA Ops:
  0.0 59.8 %mixer.1.src = bf16[512,512]{1,0:T(8,128)(2,1)} custom-call(bf16[2,128]{1,0:T(2,128)(2,1)} %bitcast.13, bf16[2,128]{1,0:T(2,128)(2,1)} %bitcast.14, f32[1,4096]{1,0:T(1,128)} %bitcast.12, f32[1,128]{1,0:T(1,128)} %bitcast.15, f32[2,16]{1,0:T(2,128)} %write_bias_ref.1, f32[2,16]{1,0:T(2,128)} %decay_bias_ref.1, f32[2,16]{1,0:T(2,128)} %log_rate_ref.1, ...), custom_call_target="tpu_custom_call" | custom-call | tf_op jit(solution)/shard_map/mixer/pallas_call | solution.py:705
  59.8 1.8 %deliver.1 = bf16[512,512]{1,0:T(8,128)(2,1)} custom-call(bf16[512,512]{1,0:T(8,128)(2,1)} %mixer.1.src), custom_call_target="tpu_custom_call" | custom-call | tf_op jit(solution)/shard_map/deliver/pallas_call | solution.py:782

commit v5 on v4

--- a/solution.py
+++ b/solution.py
@@ -1,4 +1,5 @@
 import functools
+import math
 
 import jax
 import jax.numpy as jnp
@@ -266,7 +267,10 @@
     width = mod_w.shape[2]
     half = width // 2
     total_tokens = tokens + ctx_tokens
-    rings = [lax.rem(me + r, sp) for r in range(1, sp)]
+    side = math.isqrt(sp)
+    steps = [(dz, dx) for dz in range(side) for dx in range(side) if dz + dx > 0]
+    steps.sort(key=lambda step: -sum(min(d, side - d) for d in step))
+    rings = [lax.rem(me // side + dz, side) * side + lax.rem(lax.rem(me, side) + dx, side) for dz, dx in steps]
     near = on_mesh(sp=rings[0])
     cross = [lax.rem(col + r, tp) for r in range(1, tp)]
     greet([on_mesh(sp=place) for place in rings] + [on_mesh(tp=place) for place in cross])
@@ -528,7 +532,8 @@
         def _():
             run_chain()
 
-    mid = tokens // 2
+    parts = 2
+    mid = tokens // parts
 
     def piece(head, place, part):
         return got_o.at[head, place, pl.ds(part * mid, mid)]
@@ -546,7 +551,7 @@
         )
 
     def forward(head, part):
-        src, dst = (down, up) if part == 0 else (up, down)
+        src, dst = (down, up) if part < parts // 2 else (up, down)
         return send(
             piece(head, src, part), piece(head, src, part), sent_o.at[head], recv_f.at[head, part],
             on_mesh(tp=dst),
@@ -571,17 +576,16 @@
         combined = o_v[head] + mm_t(e_v[head], jnp.concatenate(pair, axis=1))
         norm = lax.rsqrt(jnp.mean(combined * combined, axis=1, keepdims=True) + epsilon)
         got_o[head, col] = (combined * norm * head_gain_ref[...]).astype(bf16)
-        for copy in (to_up(head, 0), to_down(head, 1), to_up(head, 1), to_down(head, 0)):
-            copy.start()
+        for part in range(parts):
+            to_up(head, part).start()
+            to_down(head, parts - 1 - part).start()
         relay(head, 0, got_o.at[head, col]).start()
 
     def near_arrivals(head):
-        waits = (
-            (down, 0, recv_dn, 1, True),
-            (up, 1, recv_up, 2, True),
-            (down, 1, recv_dn, 1, False),
-            (up, 0, recv_up, 2, False),
-        )
+        waits = []
+        for part in range(parts):
+            waits.append((down, part, recv_dn, 1, part < parts // 2))
+            waits.append((up, parts - 1 - part, recv_up, 2, part < parts // 2))
         for place, part, sems, n, onward in waits:
             spot = piece(head, place, part)
             arrived(spot, sems.at[head, part])
@@ -590,7 +594,8 @@
             relay(head, n, spot).start()
 
     def far_arrivals(head):
-        for part in range(2):
+        for n in range(parts):
+            part = n // 2 if n % 2 == 0 else parts - 1 - n // 2
             spot = piece(head, far, part)
             arrived(spot, recv_f.at[head, part])
             relay(head, 3, spot).start()

time: 61.9 us -> 60.7 us (0.981)
  Pallas kernels: 61.6 us -> 60.4 us
    pallas_call x1, Pallas kernels: 59.8 us -> 58.5 us  [body(): pl.pallas_call(functools.partial(mixer_kernel, sp, tp, heads, tokens, ctx...]
where the time goes in v5:
time: 60.7 us; the launch traced here: 60.5 us
  Pallas kernels  60.4 us (100%)
    pallas_call x1, Pallas kernels, body(): pl.pallas_call(functools.partial(mixer_kernel, sp, tp, heads, tokens, ctx...  58.5 us
    pallas_call x1, Pallas kernels, body(): pl.pallas_call(deliver_kernel, in_specs=[pl.BlockSpec(memory_space=pltpu....  1.82 us

profile of v5, /device:TPU:1, one launch (start us, length us, event | category | flops | bytes accessed | tf_op | source)
XLA Modules:
  0.0 60.5 jit_solution(9675728501182185903)
XLA Ops:
  0.0 58.5 %mixer.1.src = bf16[512,512]{1,0:T(8,128)(2,1)} custom-call(bf16[2,128]{1,0:T(2,128)(2,1)} %bitcast.13, bf16[2,128]{1,0:T(2,128)(2,1)} %bitcast.14, f32[1,4096]{1,0:T(1,128)} %bitcast.12, f32[1,128]{1,0:T(1,128)} %bitcast.15, f32[2,16]{1,0:T(2,128)} %write_bias_ref.1, f32[2,16]{1,0:T(2,128)} %decay_bias_ref.1, f32[2,16]{1,0:T(2,128)} %log_rate_ref.1, ...), custom_call_target="tpu_custom_call" | custom-call | tf_op jit(solution)/shard_map/mixer/pallas_call | solution.py:710
  58.5 1.8 %deliver.1 = bf16[512,512]{1,0:T(8,128)(2,1)} custom-call(bf16[512,512]{1,0:T(8,128)(2,1)} %mixer.1.src), custom_call_target="tpu_custom_call" | custom-call | tf_op jit(solution)/shard_map/deliver/pallas_call | solution.py:787

commit v6 on v5

--- a/solution.py
+++ b/solution.py
@@ -243,10 +243,11 @@
 
 def mixer_kernel(
     sp, tp, heads, tokens, ctx_tokens,
-    cond_ref, ctx_cond_ref, gain_ref, head_gain_ref, write_bias_ref, decay_bias_ref, log_rate_ref,
+    cond_hbm, ctx_cond_hbm, gain_hbm, head_gain_hbm, write_bias_hbm, decay_bias_hbm, log_rate_hbm,
     latent_hbm, context_hbm, shift_hbm, scale_hbm, gate_hbm, query_hbm, key_hbm, value_hbm,
     write_hbm, decay_hbm, out_hbm,
     out_ref,
+    cond_ref, ctx_cond_ref, gain_ref, head_gain_ref, write_bias_ref, decay_bias_ref, log_rate_ref,
     rows_v, mod_w, q_w, k_w, v_w, gate_w, out_w, st, stats, mod_v, q_v, k_v, v_v, rate_v, run_v, run_t,
     got_p, blocks, gate_row, ctx_state, o_v, e_v, maps_m, maps_b, got_m, got_b, starts, back, got_o, acc,
     load, sent_p, recv_p, sent_t, recv_t, sent_m, recv_m, sent_b, recv_b, sent_s, recv_s,
@@ -272,7 +273,12 @@
     steps.sort(key=lambda step: -sum(min(d, side - d) for d in step))
     rings = [lax.rem(me // side + dz, side) * side + lax.rem(lax.rem(me, side) + dx, side) for dz, dx in steps]
     near = on_mesh(sp=rings[0])
-    cross = [lax.rem(col + r, tp) for r in range(1, tp)]
+    cross = [
+        lax.rem(col // 2 + dc, tp // 2) * 2 + lax.rem(col + dk, 2)
+        for dc in (2, 1, 3, 0)
+        for dk in range(2)
+        if dc + dk > 0
+    ]
     greet([on_mesh(sp=place) for place in rings] + [on_mesh(tp=place) for place in cross])
 
     def arrived(spot, sem):
@@ -287,7 +293,8 @@
         return copy
 
     gates_rows = write_hbm.shape[0]
-    mod_loads = [fetch(n, src, mod_w.at[n]) for n, src in enumerate((shift_hbm, scale_hbm, gate_hbm))]
+    mod_loads = [fetch(11, cond_hbm, cond_ref), fetch(12, ctx_cond_hbm, ctx_cond_ref)]
+    mod_loads += [fetch(n, src, mod_w.at[n]) for n, src in enumerate((shift_hbm, scale_hbm, gate_hbm))]
     row_loads = [
         fetch(3, latent_hbm, rows_v.at[pl.ds(0, tokens)]),
         fetch(4, context_hbm, rows_v.at[pl.ds(tokens, ctx_tokens)]),
@@ -300,6 +307,15 @@
         fetch(9, query_hbm, q_w),
     ]
     out_load = fetch(10, out_hbm, out_w)
+    small_loads = [
+        fetch(13, gain_hbm, gain_ref),
+        fetch(14, head_gain_hbm, head_gain_ref),
+        fetch(15, write_bias_hbm, write_bias_ref),
+        fetch(16, decay_bias_hbm, decay_bias_ref),
+        fetch(17, log_rate_hbm, log_rate_ref),
+    ]
+    for copy in mod_loads:
+        copy.wait()
 
     def silu(ref):
         value = ref[...].astype(f32)
@@ -315,8 +331,6 @@
             ).astype(bf16)
         )
     silu_rows = jnp.concatenate(lefts, axis=1)
-    for copy in mod_loads:
-        copy.wait()
     shift = jnp.dot(silu_rows, mod_w[0], preferred_element_type=f32)
     scale = jnp.dot(silu_rows, mod_w[1], preferred_element_type=f32)
     gate = jnp.dot(silu_rows, mod_w[2], preferred_element_type=f32)
@@ -327,7 +341,7 @@
         send(got_p.at[me], got_p.at[me], sent_p, recv_p, on_mesh(sp=place)).start()
 
     gate_w[2 * gates_rows :, :] = jnp.zeros((gate_w.shape[0] - 2 * gates_rows, gate_w.shape[1]), bf16)
-    for copy in row_loads:
+    for copy in row_loads + small_loads:
         copy.wait()
 
     def measure_rows(i, unused):
@@ -703,16 +717,22 @@
     rows = HEAD_DIM // split
     chunks = sum(len(part) for part in spans(tokens, ctx_tokens))
     vmem = pl.BlockSpec(memory_space=pltpu.VMEM)
-    smem = pl.BlockSpec(memory_space=pltpu.SMEM)
     anywhere = pl.BlockSpec(memory_space=pltpu.HBM)
     dma = pltpu.SemaphoreType.DMA
     flat = [jnp.transpose(w, (1, 2, 0)).reshape(-1, features) for w in (write_weight, decay_weight)]
     updated = pl.pallas_call(
         functools.partial(mixer_kernel, sp, tp, heads, tokens, ctx_tokens),
-        in_specs=[vmem] * 4 + [smem] * 3 + [anywhere] * 11,
+        in_specs=[anywhere] * 18,
         out_specs=vmem,
         out_shape=jax.ShapeDtypeStruct((tokens, width), bf16),
         scratch_shapes=[
+            pltpu.VMEM((condition.shape[0] // HEAD_DIM, HEAD_DIM), bf16),
+            pltpu.VMEM((condition.shape[0] // HEAD_DIM, HEAD_DIM), bf16),
+            pltpu.VMEM((1, features), f32),
+            pltpu.VMEM((1, HEAD_DIM), f32),
+            pltpu.SMEM(write_bias.shape, f32),
+            pltpu.SMEM(decay_bias.shape, f32),
+            pltpu.SMEM(log_rate.shape, f32),
             pltpu.VMEM((total, features), bf16),
             pltpu.VMEM((3,) + shift_weight.shape, bf16),
             pltpu.VMEM(query_weight.shape, bf16),
@@ -743,7 +763,7 @@
             pltpu.VMEM((items * split, rows, HEAD_DIM), bf16),
             pltpu.VMEM((heads, tp, tokens, HEAD_DIM), bf16),
             pltpu.VMEM((tokens, width), f32),
-            dma((11,)),
+            dma((18,)),
             dma,
             dma,
             dma,

time: 60.7 us -> 59.8 us (0.985)
  Pallas kernels: 60.4 us -> 59.5 us
    pallas_call x1, Pallas kernels: 58.5 us -> 57.7 us  [body(): pl.pallas_call(functools.partial(mixer_kernel, sp, tp, heads, tokens, ctx...]
where the time goes in v6:
time: 59.8 us; the launch traced here: 59.7 us
  Pallas kernels  59.5 us (99%)
    pallas_call x1, Pallas kernels, body(): pl.pallas_call(functools.partial(mixer_kernel, sp, tp, heads, tokens, ctx...  57.7 us
    pallas_call x1, Pallas kernels, body(): pl.pallas_call(deliver_kernel, in_specs=[pl.BlockSpec(memory_space=pltpu....  1.82 us

profile of v6, /device:TPU:1, one launch (start us, length us, event | category | flops | bytes accessed | tf_op | source)
XLA Modules:
  0.0 59.7 jit_solution(5332350659508593928)
XLA Ops:
  0.0 57.7 %mixer.1.src = bf16[512,512]{1,0:T(8,128)(2,1)} custom-call(bf16[2,128]{1,0:T(2,128)(2,1)} %bitcast.13, bf16[2,128]{1,0:T(2,128)(2,1)} %bitcast.14, f32[1,4096]{1,0:T(1,128)} %bitcast.12, f32[1,128]{1,0:T(1,128)} %bitcast.15, f32[2,16]{1,0:T(2,128)} %write_bias_hbm.1, f32[2,16]{1,0:T(2,128)} %decay_bias_hbm.1, f32[2,16]{1,0:T(2,128)} %log_rate_hbm.1, ...), custom_call_target="tpu_custom_call" | custom-call | tf_op jit(solution)/shard_map/mixer/pallas_call | solution.py:723
  57.7 1.8 %deliver.1 = bf16[512,512]{1,0:T(8,128)(2,1)} custom-call(bf16[512,512]{1,0:T(8,128)(2,1)} %mixer.1.src), custom_call_target="tpu_custom_call" | custom-call | tf_op jit(solution)/shard_map/deliver/pallas_call | solution.py:807

commit v7 on v6

--- a/solution.py
+++ b/solution.py
@@ -609,17 +609,17 @@
 
     def far_arrivals(head):
         for n in range(parts):
-            part = n // 2 if n % 2 == 0 else parts - 1 - n // 2
+            part = n
             spot = piece(head, far, part)
             arrived(spot, recv_f.at[head, part])
-            relay(head, 3, spot).start()
+            relay(head, 3 + n // (parts // 2), spot).start()
 
     def from_partner(head, n):
         arrived(got_o.at[head, 0], recv_c.at[head, n])
 
-    def add(head, place, first=False):
+    def product(head, place, rows):
         even = place - core
-        lanes = jnp.concatenate([got_o[head, even], got_o[head, even + 1]], axis=1)
+        lanes = jnp.concatenate([got_o[head, even, rows, :], got_o[head, even + 1, rows, :]], axis=1)
         depth = heads * HEAD_DIM
         weights = jnp.concatenate(
             [
@@ -628,7 +628,10 @@
             ],
             axis=0,
         )
-        part = jnp.dot(lanes, weights, preferred_element_type=f32)
+        return jnp.dot(lanes, weights, preferred_element_type=f32)
+
+    def add(head, place, first=False):
+        part = product(head, place, slice(0, tokens))
         acc[...] = part if first else acc[...] + part
 
     out_load.wait()
@@ -645,11 +648,16 @@
             from_partner(head, n)
             add(head, place)
         far_arrivals(head)
-    for head in range(heads):
-        from_partner(head, 3)
+    for head in range(heads - 1):
+        for n in range(parts):
+            arrived(piece(head, 0, 0), recv_c.at[head, 3 + n])
         add(head, far)
     lanes = pl.ds(pl.multiple_of(col * width, width), width)
-    out_ref[...] = (rows_v[0:tokens, lanes].astype(f32) + gate_row[...] * acc[...]).astype(bf16)
+    for n in range(parts):
+        arrived(piece(heads - 1, 0, 0), recv_c.at[heads - 1, 3 + n])
+        rows = slice(n * mid, (n + 1) * mid)
+        part = acc[rows, :] + product(heads - 1, far, rows)
+        out_ref[rows, :] = (rows_v[rows, lanes].astype(f32) + gate_row[...] * part).astype(bf16)
     left(got_p.at[pl.ds(0, sp - 1)], sent_p)
     left(blocks.at[pl.ds(0, tp - 1)], sent_t)
 
@@ -778,7 +786,7 @@
             dma((heads, 2)),
             dma((heads, 2)),
             dma((heads, 2)),
-            dma((heads, 4)),
+            dma((heads, 5)),
         ],
         compiler_params=pltpu.CompilerParams(
             collective_id=0, has_side_effects=True, vmem_limit_bytes=58 * 1024 * 1024

time: 59.8 us -> 59.9 us (level)
  no operation moved by 1% of the time
where the time goes in v7:
time: 59.9 us; the launch traced here: 59.7 us
  Pallas kernels  59.6 us (99%)
    pallas_call x1, Pallas kernels, body(): pl.pallas_call(functools.partial(mixer_kernel, sp, tp, heads, tokens, ctx...  57.8 us
    pallas_call x1, Pallas kernels, body(): pl.pallas_call(deliver_kernel, in_specs=[pl.BlockSpec(memory_space=pltpu....  1.82 us

profile of v7, /device:TPU:1, one launch (start us, length us, event | category | flops | bytes accessed | tf_op | source)
XLA Modules:
  0.0 59.7 jit_solution(1696707507396822092)
XLA Ops:
  0.0 57.8 %mixer.1.src = bf16[512,512]{1,0:T(8,128)(2,1)} custom-call(bf16[2,128]{1,0:T(2,128)(2,1)} %bitcast.13, bf16[2,128]{1,0:T(2,128)(2,1)} %bitcast.14, f32[1,4096]{1,0:T(1,128)} %bitcast.12, f32[1,128]{1,0:T(1,128)} %bitcast.15, f32[2,16]{1,0:T(2,128)} %write_bias_hbm.1, f32[2,16]{1,0:T(2,128)} %decay_bias_hbm.1, f32[2,16]{1,0:T(2,128)} %log_rate_hbm.1, ...), custom_call_target="tpu_custom_call" | custom-call | tf_op jit(solution)/shard_map/mixer/pallas_call | solution.py:731
  57.8 1.8 %deliver.1 = bf16[512,512]{1,0:T(8,128)(2,1)} custom-call(bf16[512,512]{1,0:T(8,128)(2,1)} %mixer.1.src), custom_call_target="tpu_custom_call" | custom-call | tf_op jit(solution)/shard_map/deliver/pallas_call | solution.py:815
